TPU v7x, 32 devices: a whole 2x2x4 slice. The times are simulated.
32 devices in a mesh: grp: 2 (over y), sp: 8 (over z, core), tp: 2 (over x).
Axes of the slice: x: 2, y: 2, z: 4, core: 2. Of those that a mesh axis runs over, the one named last changes fastest.
Arguments:
- queries_a: bfloat16 [4096, 2, 512], P(('grp', 'sp'), None, 'tp'), parts along dimension 0, may hold values from -120 to 120
- keys_a: bfloat16 [4096, 2, 512], P(('grp', 'sp'), None, 'tp'), parts along dimension 0, may hold values from -6 to 6
- values_a: bfloat16 [4096, 1024], P(('grp', 'sp'), 'tp'), parts along dimension 0, may hold values from -6 to 6
- queries_b: bfloat16 [4096, 2, 512], P(('grp', 'sp'), None, 'tp'), parts along dimension 0, may hold values from -120 to 120
- keys_b: bfloat16 [4096, 2, 512], P(('grp', 'sp'), None, 'tp'), parts along dimension 0, may hold values from -6 to 6
- values_b: bfloat16 [4096, 1024], P(('grp', 'sp'), 'tp'), parts along dimension 0, may hold values from -6 to 6
- lambdas: float32 [12], replicated, may hold values from 0.3 to 0.8
- head_gain_a: float32 [256], replicated, may hold values from 0.1 to 1.9
- head_gain_b: float32 [128], replicated, may hold values from 0.1 to 1.9
- out_a: bfloat16 [1024, 2048], P('tp'), may hold values from -0.125 to 0.125
- out_b: bfloat16 [1024, 2048], P('tp'), may hold values from -0.125 to 0.125
- residual: bfloat16 [4096, 2048], P(('grp', 'sp', 'tp')), parts along dimension 0, may hold values from -6 to 6
- gain_mix: float32 [2048], replicated, may hold values from 0.1 to 1.9
- gain_pre: float32 [2048], replicated, may hold values from 0.1 to 1.9
- gain_post: float32 [2048], replicated, may hold values from 0.1 to 1.9
- routes: int32 [4096, 4], P(('grp', 'sp', 'tp')), parts along dimension 0, may hold values from 0 to 7, all different within a row; in each aligned block of 128 rows (0 to 127, 128 to 255, ...) at most 80 rows name the same one
- route_weights: float32 [4096, 4], P(('grp', 'sp', 'tp')), parts along dimension 0, may hold values from 0.05 to 1
- expert_gate: bfloat16 [8, 2048, 2048], P('sp', None, 'tp'), may hold values from -1 to 1
- expert_up: bfloat16 [8, 2048, 2048], P('sp', None, 'tp'), may hold values from -1 to 1
- expert_down: bfloat16 [8, 2048, 2048], P('sp', 'tp'), may hold values from -0.125 to 0.125
Outputs:
- layer_out: bfloat16 [4096, 2048], P(('grp', 'sp', 'tp')), parts along dimension 0
There are 2 independent parts, one for each index of `grp`. A program takes and returns all parts, laid end to end along the dimension named above; an argument that names none is the same for every part. Nothing has to cross between parts.
Inputs may be any that keep to these rules, and one draw needn't show every extreme that they name: `routes`: in each aligned block of 128 rows (the rows of one device) no expert is named by more than 80 rows, a bound that some blocks reach.
All inputs are finite; a program needn't handle non-finite values.
Results may differ from a plain program's by a relative error of at most 0.018.
Values may be sent and summed in bfloat16 or wider, within the bound.
A program may use at most 128 MiB of HBM per device.

v0:
```python
import jax
import jax.numpy as jnp
from jax import lax
from jax.sharding import PartitionSpec as P

HA = 4
DA = 128
DB = 64


def rms_norm(values, gain_vec):
    return values * lax.rsqrt(jnp.mean(values * values, -1, keepdims=True) + 1e-06) * gain_vec


def attend(current, query_rows, key_rows, value_rows, first_row, query_pos, head_size):
    run_max, run_sum, run_acc = current
    key_count = key_rows.shape[0]
    heads = query_rows.shape[2]
    key_view = key_rows.reshape(key_count, 2, heads, head_size)
    value_view = value_rows.reshape(key_count, heads, 2 * head_size)
    key_pos = first_row + jnp.arange(key_count, dtype=jnp.int32)
    visible = (key_pos[None, :] <= query_pos[:, None])[None, :, None, :]
    scores = jnp.einsum(
        "qmhd,kmhd->mqhk", query_rows, key_view, preferred_element_type=jnp.float32
    ) * head_size ** (-0.5)
    scores = jnp.where(visible, scores, -1e30)
    new_max = jnp.maximum(run_max, jnp.max(scores, -1))
    exp_terms = jnp.where(visible, jnp.exp(scores - new_max[..., None]), 0.0)
    rescale = jnp.exp(run_max - new_max)
    run_sum = run_sum * rescale + jnp.sum(exp_terms, -1)
    run_acc = run_acc * rescale[..., None] + jnp.einsum(
        "mqhk,khe->mqhe",
        exp_terms.astype(jnp.bfloat16),
        value_view,
        preferred_element_type=jnp.float32,
    )
    return (new_max, run_sum, run_acc)


def fresh_state(length, heads, head_size):
    return (
        jnp.full((2, length, heads), -1e30, jnp.float32),
        jnp.zeros((2, length, heads), jnp.float32),
        jnp.zeros((2, length, heads, 2 * head_size), jnp.float32),
    )


def finish(current, weights_two, gain_vec):
    run_max, run_sum, run_acc = current
    mixture = (
        run_acc[0] / run_sum[0][..., None]
        - weights_two[None, :, None] * run_acc[1] / run_sum[1][..., None]
    )
    normed = rms_norm(mixture, gain_vec)
    return normed.reshape(normed.shape[0], -1).astype(jnp.bfloat16)


def slot_numbers(flat_ids, experts):
    onehot = (flat_ids[:, None] == jnp.arange(experts, dtype=jnp.int32)[None, :]).astype(jnp.int32)
    before = jnp.cumsum(onehot, 0) - onehot
    return jnp.sum(before * onehot, 1)


def send_matrix(route_rows, experts, capacity):
    groups, sub_rows, top_count = route_rows.shape
    slot_ids = jax.vmap(lambda flat_ids: slot_numbers(flat_ids, experts))(
        route_rows.reshape(groups, -1)
    )
    group_ids = jnp.arange(groups, dtype=jnp.int32)[:, None]
    row_ids = (
        route_rows.reshape(groups, -1) * (groups * capacity) + group_ids * capacity + slot_ids
    ).reshape(-1)
    col_ids = jnp.broadcast_to(
        group_ids[:, :, None] * sub_rows + jnp.arange(sub_rows, dtype=jnp.int32)[None, :, None],
        route_rows.shape,
    ).reshape(-1)
    row_hot = (
        row_ids[:, None] == jnp.arange(experts * groups * capacity, dtype=jnp.int32)[None, :]
    ).astype(jnp.bfloat16)
    col_hot = (col_ids[:, None] == jnp.arange(groups * sub_rows, dtype=jnp.int32)[None, :]).astype(
        jnp.bfloat16
    )
    return jnp.einsum("ar,ac->rc", row_hot, col_hot, preferred_element_type=jnp.float32).astype(
        jnp.bfloat16
    )


def back_matrix(route_rows, route_weights, experts, capacity):
    sub_rows, top_count = route_rows.shape
    slot_ids = slot_numbers(route_rows.reshape(-1), experts)
    row_ids = route_rows.reshape(-1) * capacity + slot_ids
    col_ids = jnp.repeat(jnp.arange(sub_rows, dtype=jnp.int32), top_count)
    row_hot = (row_ids[:, None] == jnp.arange(experts * capacity, dtype=jnp.int32)[None, :]).astype(
        jnp.float32
    )
    tok_weighted = (col_ids[:, None] == jnp.arange(sub_rows, dtype=jnp.int32)[None, :]).astype(
        jnp.float32
    ) * route_weights.reshape(-1)[:, None]
    return jnp.einsum("at,ar->tr", tok_weighted, row_hot, precision=lax.Precision.HIGHEST)


def per_device(
    queries_a,
    keys_a,
    values_a,
    queries_b,
    keys_b,
    values_b,
    lambdas,
    head_gain_a,
    head_gain_b,
    out_a,
    out_b,
    residual,
    gain_mix,
    gain_pre,
    gain_post,
    routes,
    route_weights,
    expert_gate,
    expert_up,
    expert_down,
):
    length = queries_a.shape[0]
    heads_a = queries_a.shape[2] // DA
    heads_b = queries_b.shape[2] // DB
    head_slot = lax.axis_index("tp")
    seq_slot = lax.axis_index("sp")
    lambda_a = lax.dynamic_slice_in_dim(lambdas, head_slot * heads_a, heads_a)
    lambda_b = lax.dynamic_slice_in_dim(lambdas, HA + head_slot * heads_b, heads_b)
    groups = [
        (
            queries_a.reshape(length, 2, heads_a, DA),
            queries_b.reshape(length, 2, heads_b, DB),
            seq_slot * length + jnp.arange(length, dtype=jnp.int32),
            seq_slot * length + length - 1,
        )
    ]
    initial = tuple(
        (
            (
                fresh_state(group[2].shape[0], heads_a, DA),
                fresh_state(group[2].shape[0], heads_b, DB),
            )
            for group in groups
        )
    )
    pieces = (
        lax.all_gather(keys_a, "sp", axis=0, tiled=True),
        lax.all_gather(values_a, "sp", axis=0, tiled=True),
        lax.all_gather(keys_b, "sp", axis=0, tiled=True),
        lax.all_gather(values_b, "sp", axis=0, tiled=True),
    )
    key_count = pieces[0].shape[0]
    span_rows = 1024

    def one_span(span_index, carried):
        offset = span_index * span_rows
        parts = tuple(
            (lax.dynamic_slice_in_dim(piece_part, offset, span_rows, 0) for piece_part in pieces)
        )
        group_qa, group_qb, group_pos, group_last = groups[0]

        def compute(inner, group_qa=group_qa, group_qb=group_qb, group_pos=group_pos):
            return (
                attend(inner[0], group_qa, parts[0], parts[1], offset, group_pos, DA),
                attend(inner[1], group_qb, parts[2], parts[3], offset, group_pos, DB),
            )

        updated = [lax.cond(offset <= group_last, compute, lambda inner: inner, carried[0])]
        return tuple(updated)

    final_state = lax.fori_loop(0, key_count // span_rows, one_span, initial)
    heads_out_a = finish(final_state[0][0], lambda_a, head_gain_a)
    heads_out_b = finish(final_state[0][1], lambda_b, head_gain_b)
    mixed_rows = lax.psum_scatter(
        (
            jnp.dot(heads_out_a, out_a, preferred_element_type=jnp.float32)
            + jnp.dot(heads_out_b, out_b, preferred_element_type=jnp.float32)
        ).astype(jnp.bfloat16),
        "tp",
        scatter_dimension=0,
        tiled=True,
    ).astype(jnp.float32)
    after_mix = (residual.astype(jnp.float32) + rms_norm(mixed_rows, gain_mix)).astype(jnp.bfloat16)
    normed = rms_norm(after_mix.astype(jnp.float32), gain_pre).astype(jnp.bfloat16)
    experts = lax.axis_size("sp")
    sub_rows = residual.shape[0]
    top_count = routes.shape[1]
    capacity = min(sub_rows, (5 * sub_rows * top_count + 4 * experts - 1) // (4 * experts))
    width = residual.shape[1]
    outgoing = jnp.dot(
        send_matrix(routes[None], experts, capacity), normed, preferred_element_type=jnp.float32
    ).astype(jnp.bfloat16)
    outgoing = outgoing.reshape(experts, capacity, width)
    arrived = lax.all_to_all(outgoing, "sp", split_axis=0, concat_axis=0, tiled=True)
    sources, slot_count, columns = arrived.shape
    piece_rows = lax.all_gather(arrived.reshape(-1, columns), "tp", axis=0, tiled=True)
    gate_pre = jnp.dot(piece_rows, expert_gate[0], preferred_element_type=jnp.float32)
    up_pre = jnp.dot(piece_rows, expert_up[0], preferred_element_type=jnp.float32)
    glu_part = jnp.minimum(gate_pre, 7.0)
    lin_part = jnp.clip(up_pre, -7.0, 7.0)
    hidden = (glu_part * jax.nn.sigmoid(1.702 * glu_part) * (lin_part + 1.0)).astype(jnp.bfloat16)
    partials = jnp.dot(hidden, expert_down[0], preferred_element_type=jnp.float32)
    mine = lax.psum_scatter(partials.astype(jnp.bfloat16), "tp", scatter_dimension=0, tiled=True)
    results = mine.reshape(sources, slot_count, columns)
    returned = lax.all_to_all(results, "sp", split_axis=0, concat_axis=0, tiled=True)
    combine = back_matrix(routes, route_weights, experts, capacity)
    routed = jnp.dot(
        combine,
        returned.reshape(-1, width).astype(jnp.float32),
        precision=lax.Precision.HIGHEST,
        preferred_element_type=jnp.float32,
    )
    return (after_mix.astype(jnp.float32) + rms_norm(routed, gain_post)).astype(jnp.bfloat16)


def solution(mesh):
    in_specs = (
        P(("grp", "sp"), None, "tp"),
        P(("grp", "sp"), None, "tp"),
        P(("grp", "sp"), "tp"),
        P(("grp", "sp"), None, "tp"),
        P(("grp", "sp"), None, "tp"),
        P(("grp", "sp"), "tp"),
        P(),
        P(),
        P(),
        P("tp", None),
        P("tp", None),
        P(("grp", "sp", "tp"), None),
        P(),
        P(),
        P(),
        P(("grp", "sp", "tp"), None),
        P(("grp", "sp", "tp"), None),
        P("sp", None, "tp"),
        P("sp", None, "tp"),
        P("sp", "tp", None),
    )
    out_specs = P(("grp", "sp", "tp"), None)
    return jax.shard_map(
        per_device, mesh=mesh, in_specs=in_specs, out_specs=out_specs, check_vma=False
    )
```

profile of v0, /device:TPU:0, one launch (start us, length us, event | category | flops | bytes accessed | tf_op | source)
XLA Modules:
  0.0 503.5 jit_solution(3561112254705816321)
XLA Ops:
  6.6 2.0 copy.36
  8.6 1.8 copy.38
  10.5 1.8 copy.39
  12.4 1.8 copy.41
  14.3 1.1 copy.37
  15.4 0.8 copy.42
  16.3 0.9 copy.40
  17.1 0.1 dynamic_slice.58
  17.3 0.1 dynamic_slice.59
  17.5 24.9 %all-gather.6.cloned.1.call-done = bf16[2048,2,256]{0,2,1:T(8,128)(2,1)} async-done(((bf16[256,2,256]{0,2,1:T(8,128)(2,1)}), bf16[2048,2,256]{0,2,1:T(8,128)(2,1)}) %all-gather.6.cloned.1.call-update) | async-done | bytes 2097168 | tf_op jit(solution)/shard_map/all_gather | solution.py:149
  42.4 31.3 %all-gather.8.cloned.1.call-done = bf16[2048,512]{0,1:T(8,128)(2,1)} async-done(((bf16[256,512]{0,1:T(8,128)(2,1)}), bf16[2048,512]{0,1:T(8,128)(2,1)}) %all-gather.8.cloned.1.call-update) | async-done | bytes 2097168 | tf_op jit(solution)/shard_map/all_gather | solution.py:150
  73.7 31.3 %all-gather.10.cloned.1.call-done = bf16[2048,2,256]{0,2,1:T(8,128)(2,1)} async-done(((bf16[256,2,256]{0,2,1:T(8,128)(2,1)}), bf16[2048,2,256]{0,2,1:T(8,128)(2,1)}) %all-gather.10.cloned.1.call-update) | async-done | bytes 2097168 | tf_op jit(solution)/shard_map/all_gather | solution.py:151
  104.9 31.1 %all-gather.12.cloned.1.call-done = bf16[2048,512]{0,1:T(8,128)(2,1)} async-done(((bf16[256,512]{0,1:T(8,128)(2,1)}), bf16[2048,512]{0,1:T(8,128)(2,1)}) %all-gather.12.cloned.1.call-update) | async-done | bytes 2097168 | tf_op jit(solution)/shard_map/all_gather | solution.py:152
  136.0 0.1 broadcast_in_dim.113
  136.1 1.1 broadcast_in_dim.116
  137.3 13.8 %while.24 = (s32[]{:T(128)}, f32[2,256,2]{1,2,0:T(2,128)S(1)}, f32[2,256,2]{1,2,0:T(2,128)S(1)}, f32[2,256,2,256]{3,1,0,2:T(8,128)S(1)}, f32[2,256,4]{1,2,0:T(4,...) while((s32[]{:T(128)}, f32[2,256,2]{1,2,0:T(2,128)S(1)}, ...), condition=%wide.region_7.8_spmd.clone, body=%wide.region_0.7_spmd.clone.sunk | while | flops 1640242432 | bytes 83845752 | solution.py:173
  137.3 13.8 %conditional.3 = ((f32[2,256,2]{1,2,0:T(2,128)S(1)}, f32[2,256,2]{1,2,0:T(2,128)S(1)}, f32[2,256,2,256]{3,1,0,2:T(8,128)S(1)}, f32[2,256,4]{1,2,0:T(4,128)S(1)},...) conditional(s32[]{:T(128)} %convert_element_type.151, (f32[2,256,2]{1,2,0:T(2,128)S(1)}, ...), branch_computations={%region_1.0_spmd, %region_2.6_spmd} | conditional | flops 1640242432 | bytes 83844368 | solution.py:170
  137.3 0.2 broadcast_compare_fusion
  137.5 1.8 constant_dynamic-slice_fusion.1
  139.3 1.0 fusion.7
  140.3 1.2 fusion.8
  141.5 0.3 copy-done.1
  141.9 0.6 copy-done.2
  142.5 0.2 constant_dynamic-slice_fusion
  142.7 1.3 fusion.15
  144.1 1.5 fusion.2
  145.6 2.3 fusion.3
  148.0 2.0 fusion.21
  150.0 1.0 copy-done.6
  151.1 1.3 copy.43
  152.4 2.3 fusion.84
  154.7 1.4 fusion.65
  156.0 1.6 copy.45
  157.7 0.2 fusion.64
  157.9 1.5 fusion.57
  159.4 0.7 fusion.85
  160.2 0.2 fusion.51
  160.4 1.7 fusion.34
  162.2 0.1 copy.48
  162.3 0.1 reshape.307
  162.4 0.1 eq.111
  162.6 1.3 reduce-window.16
  163.9 0.2 slice_reduce_fusion
  164.1 1.1 reduce-window.14
  165.3 0.2 slice_reduce_fusion.1
  165.6 0.1 eq.104
  165.7 0.1 fusion.73
  165.8 0.1 fusion.75
  165.9 29.2 %reduce-scatter.3.cloned.1.call-done = bf16[128,2048]{1,0:T(8,128)(2,1)} async-done(((bf16[256,2048]{1,0:T(8,128)(2,1)}), bf16[128,2048]{1,0:T(8,128)(2,1)}) %reduce-scatter.3.cloned.1.call-update) | async-done | bytes 524304 | tf_op jit(solution)/shard_map/reduce_scatter | solution.py:176
  195.1 1.2 fusion.38
  196.4 1.5 fusion.42
  197.8 3.0 convolution_convert_fusion.1
  200.8 65.0 %all_to_all.10 = bf16[8,80,2048]{2,1,0:T(8,128)(2,1)} all-to-all(bf16[8,80,2048]{2,1,0:T(8,128)(2,1)} %bitcast.199), channel_id=1, replica_groups=mesh['grp'=2,'sp'=8,'tp'=2] {'sp'}, dimensions={0} | all-to-all | bytes 5242880 | tf_op jit(solution)/shard_map/all_to_all | solution.py:196
  265.9 66.6 %all-gather.14.cloned.1.call-done = bf16[1280,2048]{1,0:T(8,128)(2,1)} async-done(((bf16[640,2048]{1,0:T(8,128)(2,1)}), bf16[1280,2048]{1,0:T(8,128)(2,1)}) %all-gather.14.cloned.1.call-update) | async-done | bytes 5242896 | tf_op jit(solution)/shard_map/all_gather | solution.py:198
  332.5 10.2 %fusion.26 = f32[1280,1024]{1,0:T(8,128)} fusion(bf16[1280,2048]{1,0:T(8,128)(2,1)} %all-gather.14.cloned.1.call-done, bf16[1,2048,1024]{2,1,0:T(8,128)(2,1)} %param.41), kind=kOutput, calls=%fused_computation.34 | convolution fusion | flops 5368709120 | bytes 14680064 | tf_op jit(solution)/shard_map/dot_general | solution.py:199
  342.7 18.7 %convolution_convert_fusion = bf16[1280,2048]{1,0:T(8,128)(2,1)} fusion(bf16[1,1024,2048]{2,1,0:T(8,128)(2,1)} %param.43, f32[1280,1024]{1,0:T(8,128)} %fusion.26, bf16[1280,2048]{1,0:T(8,128)(2,1)} %all-gather.14.cloned.1.call-done, bf16[1,2048,1024]{2,1,0:T(8,128)(2,1)} %param.42), kind=kOutput, calls=%fused_computation.30 | convolution fusion | flops 10753146880 | bytes 24117248 | tf_op jit(solution)/shard_map/dot_general | solution.py:204
  361.4 65.9 %reduce-scatter.5.cloned.1.call-done = bf16[640,2048]{1,0:T(8,128)(2,1)} async-done(((bf16[1280,2048]{1,0:T(8,128)(2,1)}), bf16[640,2048]{1,0:T(8,128)(2,1)}) %reduce-scatter.5.cloned.1.call-update) | async-done | bytes 2621456 | tf_op jit(solution)/shard_map/reduce_scatter | solution.py:205
  427.3 4.7 all-to-all-start.1
  432.1 0.1 copy.47
  432.2 0.1 mul.301
  432.3 0.8 fusion.35
  433.1 59.3 %all-to-all-done.1 = bf16[8,80,2048]{2,1,0:T(8,128)(2,1)} async-done(((bf16[8,80,2048]{2,1,0:T(8,128)(2,1)}), bf16[8,80,2048]{2,1,0:T(8,128)(2,1)}, u32[]{:S(2)}, u32[]{:S(2)}) %all-to-all-start.1) | async-done | bytes 2621472 | tf_op jit(solution)/shard_map/all_to_all | solution.py:207
  492.4 3.2 multiply_reduce_fusion
  495.7 1.0 fusion.45
  (85 shorter events, 0.9 us)
Async XLA Ops:
  6.5 152.9 %copy-start = (bf16[512,2048]{1,0:T(8,128)(2,1)S(1)}, bf16[512,2048]{1,0:T(8,128)(2,1)}, u32[]{:S(2)}) copy-start(bf16[512,2048]{1,0:T(8,128)(2,1)} %param.33) | copy-start | bytes 6291460
  6.5 9.7 %copy-start.9 = (bf16[256,2,256]{2,1,0:T(2,128)(2,1)S(1)}, bf16[256,2,256]{2,1,0:T(2,128)(2,1)}, u32[]{:S(2)}) copy-start(bf16[256,2,256]{2,1,0:T(2,128)(2,1)} %param.27) | copy-start | bytes 786436
  6.5 10.6 %copy-start.15 = (f32[256]{0:T(256)S(1)}, f32[256]{0:T(256)}, u32[]{:S(2)}) copy-start(f32[256]{0:T(256)} %param.31) | copy-start | bytes 3076
  6.5 10.6 %copy-start.17 = (f32[12]{0:T(128)S(1)}, f32[12]{0:T(128)}, u32[]{:S(2)}) copy-start(f32[12]{0:T(128)} %param.30) | copy-start | bytes 148
  6.5 10.8 %copy-start.16 = (f32[128]{0:T(128)S(1)}, f32[128]{0:T(128)}, u32[]{:S(2)}) copy-start(f32[128]{0:T(128)} %param.32) | copy-start | bytes 1540
  6.5 35.8 %all-gather.6.cloned.1.call-start = ((), (), s32[]{:S(2)}) async-start(), calls=%async_computation.4 | async-start | bytes 2359296 | tf_op jit(solution)/shard_map/all_gather | solution.py:149
  8.6 65.1 %all-gather.8.cloned.1.call-start = ((), (), s32[]{:S(2)}) async-start(), calls=%async_computation.5 | async-start | bytes 2359296 | tf_op jit(solution)/shard_map/all_gather | solution.py:150
  10.5 94.5 %all-gather.10.cloned.1.call-start = ((), (), s32[]{:S(2)}) async-start(), calls=%async_computation.6 | async-start | bytes 2359296 | tf_op jit(solution)/shard_map/all_gather | solution.py:151
  12.4 123.7 %all-gather.12.cloned.1.call-start = ((), (), s32[]{:S(2)}) async-start(), calls=%async_computation.7 | async-start | bytes 2359296 | tf_op jit(solution)/shard_map/all_gather | solution.py:152
  14.3 180.8 %reduce-scatter.3.cloned.1.call-start = ((), (), s32[]{:S(2)}) async-start(), calls=%async_computation.8 | async-start | bytes 1572864 | tf_op jit(solution)/shard_map/reduce_scatter | solution.py:176
  137.5 1.8 copy-start.3
  140.3 1.6 copy-start.1
  140.3 2.2 copy-start.2
  142.5 1.6 copy-start.4
  145.6 2.4 copy-start.5
  150.0 1.0 copy-start.6
  157.7 2.7 copy-start.7
  160.2 2.0 copy-start.13
  160.2 36.2 %copy-start.8 = (bf16[128,2048]{1,0:T(8,128)(2,1)S(1)}, bf16[128,2048]{1,0:T(8,128)(2,1)}, u32[]{:S(2)}) copy-start(bf16[128,2048]{1,0:T(8,128)(2,1)} %param.35) | copy-start | bytes 1572868
  160.2 36.2 %copy-start.10 = (f32[2048]{0:T(1024)S(1)}, f32[2048]{0:T(1024)}, u32[]{:S(2)}) copy-start(f32[2048]{0:T(1024)} %param.36) | copy-start | bytes 24580
  160.4 37.4 %copy-start.11 = (f32[2048]{0:T(1024)S(1)}, f32[2048]{0:T(1024)}, u32[]{:S(2)}) copy-start(f32[2048]{0:T(1024)} %param.37) | copy-start | bytes 24580
  162.2 170.3 %all-gather.14.cloned.1.call-start = ((), (), s32[]{:S(2)}) async-start(), calls=%async_computation.9 | async-start | bytes 7864320 | tf_op jit(solution)/shard_map/all_gather | solution.py:198
  265.8 161.5 %reduce-scatter.5.cloned.1.call-start = ((), (), s32[]{:S(2)}) async-start(), calls=%async_computation.10 | async-start | bytes 7864320 | tf_op jit(solution)/shard_map/reduce_scatter | solution.py:205
  361.4 70.7 %copy-start.14 = (f32[128,4]{0,1:T(4,128)S(1)}, f32[128,4]{0,1:T(4,128)}, u32[]{:S(2)}) copy-start(f32[128,4]{0,1:T(4,128)} %param.40) | copy-start | bytes 6148
  427.3 68.3 %copy-start.12 = (f32[2048]{0:T(1024)S(1)}, f32[2048]{0:T(1024)}, u32[]{:S(2)}) copy-start(f32[2048]{0:T(1024)} %param.38) | copy-start | bytes 24580
  427.3 65.1 %all-to-all-start.1 = ((bf16[8,80,2048]{2,1,0:T(8,128)(2,1)}), bf16[8,80,2048]{2,1,0:T(8,128)(2,1)}, u32[]{:S(2)}, u32[]{:S(2)}) async-start(bf16[8,80,2048]{2,1,0:T(8,128)(2,1)} %bitcast.202), calls=%async_computation.3 | async-start | bytes 5242880 | tf_op jit(solution)/shard_map/all_to_all | solution.py:207
Sparse Core Ops, SparseCore 0:
  8.9 33.3 all-gather.5
  44.0 29.6 all-gather.7
  75.3 29.6 all-gather.9
  106.4 29.6 all-gather.11
  162.3 32.7 reduce-scatter.2
  266.0 66.4 all-gather.13
  361.5 65.7 reduce-scatter.4
where the time goes:
time: 504 us
  waiting for transfers between devices  340 us (67%)
  blocking collectives  65 us (13%)
  matrix products  44.2 us (9%)
  local copies, waits for them, and re-layouts  22.1 us (4%)
  between operations  13.8 us (3%)
  other arithmetic  13.5 us (3%)
  starting transfers between devices  5.04 us (1%)
    all_gather x1, waiting for transfers between devices, per_device(): lax.all_gather(arrived.reshape(-1, columns), 'tp', axis=0, tiled=True)  66.6 us
    reduce_scatter x1, waiting for transfers between devices, per_device(): lax.psum_scatter(partials.astype(jnp.bfloat16), 'tp', scatter_dimension=0...  65.9 us
    all_to_all x1, blocking collectives, per_device(): lax.all_to_all(outgoing, 'sp', split_axis=0, concat_axis=0, tiled=True)  65 us
    all_to_all x1, waiting for transfers between devices, per_device(): lax.all_to_all(results, 'sp', split_axis=0, concat_axis=0, tiled=True)  59.3 us
    all_gather x1, waiting for transfers between devices, per_device(): lax.all_gather(values_a, 'sp', axis=0, tiled=True)  31.3 us
    all_gather x1, waiting for transfers between devices, per_device(): lax.all_gather(keys_b, 'sp', axis=0, tiled=True)  31.3 us
    all_gather x1, waiting for transfers between devices, per_device(): lax.all_gather(values_b, 'sp', axis=0, tiled=True)  31.1 us
    reduce_scatter x1, waiting for transfers between devices, per_device(): lax.psum_scatter((jnp.dot(heads_out_a, out_a, preferred_element_type=jnp....  29.2 us
  transfers between devices with their start and end apart: 8, of which 8 were waited for; matrix products, arithmetic and copies ran while one was open for 3% of the time, Pallas kernels for 0%

commit v1 on v0

--- a/solution.py
+++ b/solution.py
@@ -1,6 +1,8 @@
 import jax
 import jax.numpy as jnp
 from jax import lax
+from jax.experimental import pallas as pl
+from jax.experimental.pallas import tpu as pltpu
 from jax.sharding import PartitionSpec as P
 
 HA = 4
@@ -55,48 +57,283 @@
     return normed.reshape(normed.shape[0], -1).astype(jnp.bfloat16)
 
 
-def slot_numbers(flat_ids, experts):
-    onehot = (flat_ids[:, None] == jnp.arange(experts, dtype=jnp.int32)[None, :]).astype(jnp.int32)
-    before = jnp.cumsum(onehot, 0) - onehot
-    return jnp.sum(before * onehot, 1)
-
-
-def send_matrix(route_rows, experts, capacity):
-    groups, sub_rows, top_count = route_rows.shape
-    slot_ids = jax.vmap(lambda flat_ids: slot_numbers(flat_ids, experts))(
-        route_rows.reshape(groups, -1)
-    )
-    group_ids = jnp.arange(groups, dtype=jnp.int32)[:, None]
-    row_ids = (
-        route_rows.reshape(groups, -1) * (groups * capacity) + group_ids * capacity + slot_ids
-    ).reshape(-1)
-    col_ids = jnp.broadcast_to(
-        group_ids[:, :, None] * sub_rows + jnp.arange(sub_rows, dtype=jnp.int32)[None, :, None],
-        route_rows.shape,
-    ).reshape(-1)
-    row_hot = (
-        row_ids[:, None] == jnp.arange(experts * groups * capacity, dtype=jnp.int32)[None, :]
+MESH = pl.DeviceIdType.MESH
+CORES = 2
+VMEM_BYTES = 60 * 1024 * 1024
+
+
+def place():
+    sp = lax.axis_index("sp")
+    return sp // CORES, sp % CORES, lax.axis_index("tp")
+
+
+def greet(chips, tps):
+    chip, core, tp = place()
+    barrier = pltpu.get_barrier_semaphore()
+    for step in range(1, chips):
+        other = (chip + step) % chips
+        pl.semaphore_signal(
+            barrier, inc=1, device_id={"sp": other * CORES + core, "tp": tp}, device_id_type=MESH
+        )
+    for step in range(1, tps):
+        pl.semaphore_signal(
+            barrier,
+            inc=1,
+            device_id={"sp": chip * CORES + core, "tp": (tp + step) % tps},
+            device_id_type=MESH,
+        )
+    pl.semaphore_signal(
+        barrier, inc=1, device_id={"sp": chip * CORES + 1 - core, "tp": tp}, device_id_type=MESH
+    )
+    pl.semaphore_wait(barrier, chips - 1 + tps - 1 + 1)
+
+
+def gather_kernel(chips, tps, own_ref, all_ref, send_sem, recv_sem, own_sem):
+    chip, core, tp = place()
+    greet(chips, tps)
+    started = []
+
+    def block(chip_of, core_of, tp_of):
+        return (chip_of * CORES + core_of) * tps + tp_of
+
+    def send(source, index, sp_to, tp_to):
+        copy = pltpu.make_async_remote_copy(
+            src_ref=source,
+            dst_ref=all_ref.at[index],
+            send_sem=send_sem.at[len(started)],
+            recv_sem=recv_sem.at[index],
+            device_id={"sp": sp_to, "tp": tp_to},
+            device_id_type=MESH,
+        )
+        copy.start()
+        started.append(copy)
+
+    def arrived(index):
+        pltpu.make_async_copy(all_ref.at[index], all_ref.at[index], recv_sem.at[index]).wait()
+
+    own = block(chip, core, tp)
+    for step in range(1, chips):
+        send(own_ref, own, (chip + step) % chips * CORES + core, tp)
+    for step in range(1, tps):
+        send(own_ref, own, chip * CORES + core, (tp + step) % tps)
+    send(own_ref, own, chip * CORES + 1 - core, tp)
+    mine = pltpu.make_async_copy(own_ref, all_ref.at[own], own_sem)
+    mine.start()
+
+    def from_tp(chip_of):
+        for step in range(1, tps):
+            index = block(chip_of, core, (tp + step) % tps)
+            arrived(index)
+            send(all_ref.at[index], index, chip * CORES + 1 - core, tp)
+
+    for step in range(1, chips):
+        chip_of = (chip - step + chips) % chips
+        index = block(chip_of, core, tp)
+        arrived(index)
+        for tp_step in range(1, tps):
+            send(all_ref.at[index], index, chip * CORES + core, (tp + tp_step) % tps)
+        send(all_ref.at[index], index, chip * CORES + 1 - core, tp)
+        from_tp((chip - step + 1 + chips) % chips)
+    from_tp((chip + 1) % chips)
+    for step in range(chips):
+        for tp_of in range(tps):
+            arrived(block((chip - step + chips) % chips, 1 - core, (tp + tp_of) % tps))
+    mine.wait()
+    for copy in started:
+        copy.wait_send()
+
+
+def gather_rows(own, chips, tps):
+    blocks = chips * CORES * tps
+    sends = chips - 1 + tps - 1 + 1 + (chips - 1) * tps + chips * (tps - 1)
+    return pl.pallas_call(
+        lambda *refs: gather_kernel(chips, tps, *refs),
+        name="gather_rows",
+        out_shape=jax.ShapeDtypeStruct((blocks,) + own.shape, own.dtype),
+        in_specs=[pl.BlockSpec(memory_space=pl.ANY)],
+        out_specs=pl.BlockSpec(memory_space=pl.ANY),
+        scratch_shapes=[
+            pltpu.SemaphoreType.DMA((sends,)),
+            pltpu.SemaphoreType.DMA((blocks,)),
+            pltpu.SemaphoreType.DMA,
+        ],
+        compiler_params=pltpu.CompilerParams(collective_id=1, has_side_effects=True),
+    )(own)
+
+
+def add_rows(target, index, source, source_index):
+    rows = target.shape[1]
+    chunk = min(rows, 16)
+
+    @pl.loop(0, rows // chunk)
+    def _(part):
+        span = pl.ds(pl.multiple_of(part * chunk, chunk), chunk)
+        target[index, span, :] = (
+            target[index, span, :].astype(jnp.float32)
+            + source[source_index, span, :].astype(jnp.float32)
+        ).astype(target.dtype)
+
+
+def scatter_kernel(
+    chips, tps, part_ref, out_ref, acc, core_in, tp_in, chip_in, load_sem, send_sem, core_sem, tp_sem, chip_sem
+):
+    chip, core, tp = place()
+    load = []
+    started = []
+    for step in range(chips):
+        for tp_step in range(tps):
+            chip_of, tp_of = (chip + 1 + step) % chips, (tp + 1 + tp_step) % tps
+            copy = pltpu.make_async_copy(
+                part_ref.at[(chip_of * CORES + core) * tps + tp_of],
+                acc.at[chip_of * tps + tp_of],
+                load_sem.at[step * tps + tp_step],
+            )
+            copy.start()
+            load.append(copy)
+    greet(chips, tps)
+
+    def send(source, target, recv_sem, sp_to, tp_to):
+        copy = pltpu.make_async_remote_copy(
+            src_ref=source,
+            dst_ref=target,
+            send_sem=send_sem.at[len(started)],
+            recv_sem=recv_sem,
+            device_id={"sp": sp_to, "tp": tp_to},
+            device_id_type=MESH,
+        )
+        copy.start()
+        started.append(copy)
+
+    def arrived(target, index, sem):
+        pltpu.make_async_copy(target.at[index], target.at[index], sem).wait()
+
+    for step in range(chips):
+        chip_of = (chip + 1 + step) % chips
+        for tp_step in range(tps):
+            tp_of = (tp + 1 + tp_step) % tps
+            index = chip_of * tps + tp_of
+            send(
+                part_ref.at[(chip_of * CORES + 1 - core) * tps + tp_of],
+                core_in.at[index],
+                core_sem.at[index],
+                chip * CORES + 1 - core,
+                tp,
+            )
+
+    def chip_stage(step):
+        chip_of = (chip + 1 + step) % chips
+        for tp_step in range(1, tps):
+            source = (tp + tp_step) % tps
+            index = chip_of * tps + source
+            arrived(tp_in, index, tp_sem.at[index])
+            add_rows(acc, chip_of * tps + tp, tp_in, index)
+        if step < chips - 1:
+            send(
+                acc.at[chip_of * tps + tp],
+                chip_in.at[chip],
+                chip_sem.at[chip],
+                chip_of * CORES + core,
+                tp,
+            )
+
+    for step in range(chips):
+        chip_of = (chip + 1 + step) % chips
+        for tp_step in range(tps):
+            tp_of = (tp + 1 + tp_step) % tps
+            index = chip_of * tps + tp_of
+            load[step * tps + tp_step].wait()
+            arrived(core_in, index, core_sem.at[index])
+            add_rows(acc, index, core_in, index)
+            if tp_step < tps - 1:
+                send(
+                    acc.at[index],
+                    tp_in.at[chip_of * tps + tp],
+                    tp_sem.at[chip_of * tps + tp],
+                    chip * CORES + core,
+                    tp_of,
+                )
+        if step > 0:
+            chip_stage(step - 1)
+    chip_stage(chips - 1)
+    for step in range(1, chips):
+        source = (chip - step + chips) % chips
+        arrived(chip_in, source, chip_sem.at[source])
+        if step < chips - 1:
+            add_rows(acc, chip * tps + tp, chip_in, source)
+    last = (chip + 1) % chips
+    rows = out_ref.shape[0]
+    chunk = min(rows, 16)
+
+    @pl.loop(0, rows // chunk)
+    def _(part):
+        span = pl.ds(pl.multiple_of(part * chunk, chunk), chunk)
+        out_ref[span, :] = acc[chip * tps + tp, span, :].astype(jnp.float32) + chip_in[
+            last, span, :
+        ].astype(jnp.float32)
+
+    for copy in started:
+        copy.wait_send()
+
+
+def scatter_rows(parts, chips, tps):
+    blocks, rows, width = parts.shape
+    half = chips * tps
+    sends = half + chips * (tps - 1) + chips - 1
+    return pl.pallas_call(
+        lambda *refs: scatter_kernel(chips, tps, *refs),
+        name="scatter_rows",
+        out_shape=jax.ShapeDtypeStruct((rows, width), jnp.float32),
+        in_specs=[pl.BlockSpec(memory_space=pl.ANY)],
+        out_specs=pl.BlockSpec(memory_space=pltpu.VMEM),
+        scratch_shapes=[
+            pltpu.VMEM((half, rows, width), parts.dtype),
+            pltpu.VMEM((half, rows, width), parts.dtype),
+            pltpu.VMEM((half, rows, width), parts.dtype),
+            pltpu.VMEM((chips, rows, width), parts.dtype),
+            pltpu.SemaphoreType.DMA((half,)),
+            pltpu.SemaphoreType.DMA((sends,)),
+            pltpu.SemaphoreType.DMA((half,)),
+            pltpu.SemaphoreType.DMA((half,)),
+            pltpu.SemaphoreType.DMA((chips,)),
+        ],
+        compiler_params=pltpu.CompilerParams(
+            collective_id=2, has_side_effects=True, vmem_limit_bytes=VMEM_BYTES
+        ),
+    )(parts)
+
+
+def expert_parts(gathered, expert, experts, capacity, width, weights):
+    gate, up, down = weights
+    blocks, rows, _ = gathered.shape
+    shares = lax.dynamic_slice_in_dim(gathered[:, :, width:], expert, 1, 2)[:, :, 0]
+    named = shares > 0
+    order = jnp.arange(rows, dtype=jnp.int32)
+    slots = jnp.dot(
+        named.astype(jnp.bfloat16),
+        (order[:, None] < order[None, :]).astype(jnp.bfloat16),
+        preferred_element_type=jnp.float32,
+    ).astype(jnp.int32)
+    picks = (slots[:, None, :] == jnp.arange(capacity, dtype=jnp.int32)[None, :, None]) & named[:, None, :]
+    rows_in = jnp.einsum(
+        "bct,btd->bcd",
+        picks.astype(jnp.bfloat16),
+        gathered[:, :, :width],
+        preferred_element_type=jnp.float32,
     ).astype(jnp.bfloat16)
-    col_hot = (col_ids[:, None] == jnp.arange(groups * sub_rows, dtype=jnp.int32)[None, :]).astype(
-        jnp.bfloat16
-    )
-    return jnp.einsum("ar,ac->rc", row_hot, col_hot, preferred_element_type=jnp.float32).astype(
-        jnp.bfloat16
-    )
-
-
-def back_matrix(route_rows, route_weights, experts, capacity):
-    sub_rows, top_count = route_rows.shape
-    slot_ids = slot_numbers(route_rows.reshape(-1), experts)
-    row_ids = route_rows.reshape(-1) * capacity + slot_ids
-    col_ids = jnp.repeat(jnp.arange(sub_rows, dtype=jnp.int32), top_count)
-    row_hot = (row_ids[:, None] == jnp.arange(experts * capacity, dtype=jnp.int32)[None, :]).astype(
-        jnp.float32
-    )
-    tok_weighted = (col_ids[:, None] == jnp.arange(sub_rows, dtype=jnp.int32)[None, :]).astype(
-        jnp.float32
-    ) * route_weights.reshape(-1)[:, None]
-    return jnp.einsum("at,ar->tr", tok_weighted, row_hot, precision=lax.Precision.HIGHEST)
+    rows_in = rows_in.reshape(blocks * capacity, width)
+    gate_pre = jnp.dot(rows_in, gate, preferred_element_type=jnp.float32)
+    up_pre = jnp.dot(rows_in, up, preferred_element_type=jnp.float32)
+    glu_part = jnp.minimum(gate_pre, 7.0)
+    lin_part = jnp.clip(up_pre, -7.0, 7.0)
+    hidden = (glu_part * jax.nn.sigmoid(1.702 * glu_part) * (lin_part + 1.0)).astype(jnp.bfloat16)
+    outs = jnp.dot(hidden, down, preferred_element_type=jnp.float32).astype(jnp.bfloat16)
+    back = jnp.where(picks, shares[:, None, :], 0).astype(jnp.bfloat16)
+    return jnp.einsum(
+        "bct,bcd->btd",
+        back,
+        outs.reshape(blocks, capacity, width),
+        preferred_element_type=jnp.float32,
+    ).astype(jnp.bfloat16)
 
 
 def per_device(
@@ -189,29 +426,21 @@
     top_count = routes.shape[1]
     capacity = min(sub_rows, (5 * sub_rows * top_count + 4 * experts - 1) // (4 * experts))
     width = residual.shape[1]
-    outgoing = jnp.dot(
-        send_matrix(routes[None], experts, capacity), normed, preferred_element_type=jnp.float32
+    chips, tps = experts // CORES, lax.axis_size("tp")
+    extra = -(-experts // 128) * 128
+    shares = jnp.sum(
+        jnp.where(
+            routes[:, :, None] == jnp.arange(extra, dtype=jnp.int32)[None, None, :],
+            route_weights[:, :, None],
+            0.0,
+        ),
+        1,
     ).astype(jnp.bfloat16)
-    outgoing = outgoing.reshape(experts, capacity, width)
-    arrived = lax.all_to_all(outgoing, "sp", split_axis=0, concat_axis=0, tiled=True)
-    sources, slot_count, columns = arrived.shape
-    piece_rows = lax.all_gather(arrived.reshape(-1, columns), "tp", axis=0, tiled=True)
-    gate_pre = jnp.dot(piece_rows, expert_gate[0], preferred_element_type=jnp.float32)
-    up_pre = jnp.dot(piece_rows, expert_up[0], preferred_element_type=jnp.float32)
-    glu_part = jnp.minimum(gate_pre, 7.0)
-    lin_part = jnp.clip(up_pre, -7.0, 7.0)
-    hidden = (glu_part * jax.nn.sigmoid(1.702 * glu_part) * (lin_part + 1.0)).astype(jnp.bfloat16)
-    partials = jnp.dot(hidden, expert_down[0], preferred_element_type=jnp.float32)
-    mine = lax.psum_scatter(partials.astype(jnp.bfloat16), "tp", scatter_dimension=0, tiled=True)
-    results = mine.reshape(sources, slot_count, columns)
-    returned = lax.all_to_all(results, "sp", split_axis=0, concat_axis=0, tiled=True)
-    combine = back_matrix(routes, route_weights, experts, capacity)
-    routed = jnp.dot(
-        combine,
-        returned.reshape(-1, width).astype(jnp.float32),
-        precision=lax.Precision.HIGHEST,
-        preferred_element_type=jnp.float32,
-    )
+    gathered = gather_rows(jnp.concatenate([normed, shares], 1), chips, tps)
+    parts = expert_parts(
+        gathered, seq_slot, experts, capacity, width, (expert_gate[0], expert_up[0], expert_down[0])
+    )
+    routed = scatter_rows(parts, chips, tps)
     return (after_mix.astype(jnp.float32) + rms_norm(routed, gain_post)).astype(jnp.bfloat16)
 
 

time: 504 us -> 398 us (0.79)
  waiting for transfers between devices: 340 us -> 151 us
  Pallas kernels: 0 us -> 145 us
  blocking collectives: 65 us -> 0 us
    pallas_call x0 -> x2, Pallas kernels: none -> 145 us  [the longest x1 77.5 us: scatter_rows(): pl.pallas_call(lambda *refs: scatter_kernel(chips, tps, *refs), name='sca...]
    all_gather x1 -> x0, waiting for transfers between devices: 66.6 us -> none  [per_device(): lax.all_gather(arrived.reshape(-1, columns), 'tp', axis=0, tiled=True)]
    reduce_scatter x1 -> x0, waiting for transfers between devices: 65.9 us -> none  [per_device(): lax.psum_scatter(partials.astype(jnp.bfloat16), 'tp', scatter_dimension=0...]
    all_to_all x1 -> x0, blocking collectives: 65 us -> none  [per_device(): lax.all_to_all(outgoing, 'sp', split_axis=0, concat_axis=0, tiled=True)]
    all_to_all x1 -> x0, waiting for transfers between devices: 59.3 us -> none  [per_device(): lax.all_to_all(results, 'sp', split_axis=0, concat_axis=0, tiled=True)]
    unnamed x37 -> x39, local copies, waits for them, and re-layouts: 10.6 us -> 12.7 us
  transfers between devices with their start and end apart: 8 -> 5, of which waited for: 8 -> 5; matrix products, arithmetic and copies ran while one was open for 3% -> 2% of each run, Pallas kernels for 0% -> 0%
where the time goes in v1:
time: 398 us; the launch traced here: 397 us
  waiting for transfers between devices  151 us (38%)
  Pallas kernels  145 us (36%)
  matrix products  47.7 us (12%)
  local copies, waits for them, and re-layouts  24.7 us (6%)
  other arithmetic  14.7 us (4%)
  between operations  13.4 us (3%)
    pallas_call x1, Pallas kernels, scatter_rows(): pl.pallas_call(lambda *refs: scatter_kernel(chips, tps, *refs), name='sca...  77.5 us
    pallas_call x1, Pallas kernels, gather_rows(): pl.pallas_call(lambda *refs: gather_kernel(chips, tps, *refs), name='gath...  67.3 us
    reduce_scatter x1, waiting for transfers between devices, per_device(): lax.psum_scatter((jnp.dot(heads_out_a, out_a, preferred_element_type=jnp....  32.7 us
    all_gather x1, waiting for transfers between devices, per_device(): lax.all_gather(values_a, 'sp', axis=0, tiled=True)  31.4 us
    all_gather x1, waiting for transfers between devices, per_device(): lax.all_gather(keys_b, 'sp', axis=0, tiled=True)  31.3 us
    all_gather x1, waiting for transfers between devices, per_device(): lax.all_gather(values_b, 'sp', axis=0, tiled=True)  31.1 us
    all_gather x1, waiting for transfers between devices, per_device(): lax.all_gather(keys_a, 'sp', axis=0, tiled=True)  25 us
    dot_general x1, matrix products, expert_parts(): jnp.dot(hidden, down, preferred_element_type=jnp.float32)  18.7 us
  transfers between devices with their start and end apart: 5, of which 5 were waited for; matrix products, arithmetic and copies ran while one was open for 2% of the time, Pallas kernels for 0%

profile of v1, /device:TPU:0, one launch (start us, length us, event | category | flops | bytes accessed | tf_op | source)
XLA Modules:
  0.0 397.1 jit_solution(15112393547182700014)
XLA Ops:
  6.5 0.0 all-gather.5.cloned.1.call-start
  6.6 2.0 copy.58
  8.6 0.0 all-gather.7.cloned.1.call-start
  8.6 1.8 copy.60
  10.5 0.0 all-gather.9.cloned.1.call-start
  10.5 1.8 copy.61
  12.3 0.0 all-gather.11.cloned.1.call-start
  12.4 1.8 copy.63
  14.2 0.0 reduce-scatter.2.cloned.1.call-start
  14.3 1.1 copy.59
  15.4 0.8 copy.64
  16.2 0.9 copy.62
  17.1 0.1 dynamic_slice.61
  17.2 0.1 broadcast_bitcast_fusion.3
  17.3 0.1 dynamic_slice.62
  17.3 0.1 broadcast_bitcast_fusion
  17.4 25.0 %all-gather.5.cloned.1.call-done = bf16[2048,2,256]{0,2,1:T(8,128)(2,1)} async-done(((bf16[256,2,256]{0,2,1:T(8,128)(2,1)}), bf16[2048,2,256]{0,2,1:T(8,128)(2,1)}) %all-gather.5.cloned.1.call-update) | async-done | bytes 2097168 | tf_op jit(solution)/shard_map/all_gather | solution.py:386
  42.4 31.4 %all-gather.7.cloned.1.call-done = bf16[2048,512]{0,1:T(8,128)(2,1)} async-done(((bf16[256,512]{0,1:T(8,128)(2,1)}), bf16[2048,512]{0,1:T(8,128)(2,1)}) %all-gather.7.cloned.1.call-update) | async-done | bytes 2097168 | tf_op jit(solution)/shard_map/all_gather | solution.py:387
  73.8 31.3 %all-gather.9.cloned.1.call-done = bf16[2048,2,256]{0,2,1:T(8,128)(2,1)} async-done(((bf16[256,2,256]{0,2,1:T(8,128)(2,1)}), bf16[2048,2,256]{0,2,1:T(8,128)(2,1)}) %all-gather.9.cloned.1.call-update) | async-done | bytes 2097168 | tf_op jit(solution)/shard_map/all_gather | solution.py:388
  105.0 31.1 %all-gather.11.cloned.1.call-done = bf16[2048,512]{0,1:T(8,128)(2,1)} async-done(((bf16[256,512]{0,1:T(8,128)(2,1)}), bf16[2048,512]{0,1:T(8,128)(2,1)}) %all-gather.11.cloned.1.call-update) | async-done | bytes 2097168 | tf_op jit(solution)/shard_map/all_gather | solution.py:389
  136.1 0.1 broadcast_in_dim.129
  136.2 1.1 broadcast_in_dim.132
  137.3 13.7 %while.24 = (s32[]{:T(128)}, f32[2,256,2]{1,2,0:T(2,128)S(1)}, f32[2,256,2]{1,2,0:T(2,128)S(1)}, f32[2,256,2,256]{3,1,0,2:T(8,128)S(1)}, f32[2,256,4]{1,2,0:T(4,...) while((s32[]{:T(128)}, f32[2,256,2]{1,2,0:T(2,128)S(1)}, ...), condition=%wide.region_7.8_spmd.clone, body=%wide.region_0.7_spmd.clone.sunk | while | flops 1640242432 | bytes 83845752 | solution.py:410
  137.3 13.7 %conditional.3 = ((f32[2,256,2]{1,2,0:T(2,128)S(1)}, f32[2,256,2]{1,2,0:T(2,128)S(1)}, f32[2,256,2,256]{3,1,0,2:T(8,128)S(1)}, f32[2,256,4]{1,2,0:T(4,128)S(1)},...) conditional(s32[]{:T(128)} %convert_element_type.127, (f32[2,256,2]{1,2,0:T(2,128)S(1)}, ...), branch_computations={%region_1.0_spmd, %region_2.6_spmd} | conditional | flops 1640242432 | bytes 83844368 | solution.py:407
  137.3 0.2 broadcast_compare_fusion
  137.5 1.8 constant_dynamic-slice_fusion.1
  139.3 1.0 fusion.7
  140.3 1.2 fusion.8
  141.5 0.3 copy-done.1
  141.9 0.6 copy-done.2
  142.5 0.2 constant_dynamic-slice_fusion
  142.7 1.3 fusion.15
  144.1 1.5 fusion.2
  145.6 2.3 fusion.3
  148.0 2.0 fusion.21
  150.1 1.0 copy-done.7
  151.0 1.3 copy.65
  152.4 2.3 fusion.79
  154.6 1.4 fusion.64
  156.0 1.6 copy.67
  157.6 0.1 fusion.78
  157.7 0.2 fusion.63
  157.9 1.5 fusion.58
  159.4 0.7 fusion.80
  160.2 0.2 fusion.52
  160.4 1.7 fusion.39
  162.2 0.2 select_reduce_fusion
  162.4 32.7 %reduce-scatter.2.cloned.1.call-done = bf16[128,2048]{1,0:T(8,128)(2,1)} async-done(((bf16[256,2048]{1,0:T(8,128)(2,1)}), bf16[128,2048]{1,0:T(8,128)(2,1)}) %reduce-scatter.2.cloned.1.call-update) | async-done | bytes 524304 | tf_op jit(solution)/shard_map/reduce_scatter | solution.py:413
  195.0 1.2 fusion.40
  196.3 1.4 fusion.44
  197.7 0.2 fusion.46
  197.9 0.9 pad_maximum_fusion.refs_0_
  198.8 67.3 %gather_rows.1 = bf16[16,128,2176]{2,1,0:T(8,128)(2,1)} custom-call(bf16[128,2176]{1,0:T(8,128)(2,1)} %pad_maximum_fusion.refs_0_), custom_call_target="tpu_custom_call" | custom-call | tf_op jit(solution)/shard_map/gather_rows/pallas_call | solution.py:149
  266.1 1.1 slice.38
  267.2 0.4 dynamic-slice_reduce_fusion
  267.6 0.1 convolution_convert_fusion.2
  267.7 5.1 %fusion.30 = bf16[16,80,2048]{2,1,0:T(8,128)(2,1)S(1)} fusion(bf16[16,128,2176]{2,1,0:T(8,128)(2,1)} %gather_rows.1, s32[16,128]{1,0:T(8,128)S(1)} %convolution_convert_fusion.2, pred[16,128]{1,0:T(8,128)(4,1)S(1)} %broadcast_compare_fusion.1), kind=kOutput, calls=%fused_computation.39 | convolution fusion | flops 674037760 | bytes 13641728 | tf_op jit(solution)/shard_map/bct,btd->bcd/dot_general | solution.py:317
  272.8 2.4 copy-done.5
  275.2 7.4 %fusion.28 = f32[1280,1024]{1,0:T(8,128)} fusion(bf16[1280,2048]{1,0:T(8,128)(2,1)S(1)} %bitcast.174, bf16[1,2048,1024]{2,1,0:T(8,128)(2,1)S(1)} %copy-done.18), kind=kOutput, calls=%fused_computation.37 | convolution fusion | flops 5368709120 | bytes 14680064 | tf_op jit(solution)/shard_map/dot_general | solution.py:324
  282.5 18.7 %convolution_convert_fusion = bf16[1280,2048]{1,0:T(8,128)(2,1)} fusion(bf16[1,1024,2048]{2,1,0:T(8,128)(2,1)} %param.43, f32[1280,1024]{1,0:T(8,128)} %fusion.28, bf16[1280,2048]{1,0:T(8,128)(2,1)} %bitcast.175, bf16[1,2048,1024]{2,1,0:T(8,128)(2,1)} %param.42), kind=kOutput, calls=%fused_computation.32 | convolution fusion | flops 10753146880 | bytes 24117248 | tf_op jit(solution)/shard_map/dot_general | solution.py:329
  301.2 8.2 %convolution_convert_fusion.1.refs_0_ = bf16[16,128,2048]{2,1,0:T(8,128)(2,1)} fusion(bf16[16,80,2048]{2,1,0:T(8,128)(2,1)} %bitcast.176, s32[16,128]{1,0:T(8,128)S(1)} %convolution_convert_fusion.2, pred[16,128]{1,0:T(8,128)(4,1)S(1)} %broadcast_compare_fusion.1, bf16[16,128]{1,0:T(8,128)(2,1)S(1)} %dynamic-slice_reduce_fusion), kind=kOutput, calls=%fused_computation.33 | convolution fusion | flops 675774464 | bytes 13645824 | tf_op jit(solution)/shard_map/bct,bcd->btd/dot_general | solution.py:331
  309.4 77.5 %scatter_rows.1 = f32[128,2048]{1,0:T(8,128)} custom-call(bf16[16,128,2048]{2,1,0:T(8,128)(2,1)} %convolution_convert_fusion.1.refs_0_), custom_call_target="tpu_custom_call" | custom-call | tf_op jit(solution)/shard_map/scatter_rows/pallas_call | solution.py:282
  386.9 1.4 multiply_reduce_fusion
  388.3 2.2 fusion.47
  (69 shorter events, 0.3 us)
Async XLA Ops:
  6.5 152.8 %copy-start = (bf16[512,2048]{1,0:T(8,128)(2,1)S(1)}, bf16[512,2048]{1,0:T(8,128)(2,1)}, u32[]{:S(2)}) copy-start(bf16[512,2048]{1,0:T(8,128)(2,1)} %param.33) | copy-start | bytes 6291460
  6.5 9.7 %copy-start.10 = (bf16[256,2,256]{2,1,0:T(2,128)(2,1)S(1)}, bf16[256,2,256]{2,1,0:T(2,128)(2,1)}, u32[]{:S(2)}) copy-start(bf16[256,2,256]{2,1,0:T(2,128)(2,1)} %param.27) | copy-start | bytes 786436
  6.5 10.6 %copy-start.16 = (f32[256]{0:T(256)S(1)}, f32[256]{0:T(256)}, u32[]{:S(2)}) copy-start(f32[256]{0:T(256)} %param.31) | copy-start | bytes 3076
  6.5 10.6 %copy-start.19 = (f32[12]{0:T(128)S(1)}, f32[12]{0:T(128)}, u32[]{:S(2)}) copy-start(f32[12]{0:T(128)} %param.30) | copy-start | bytes 148
  6.5 10.8 %copy-start.17 = (f32[128]{0:T(128)S(1)}, f32[128]{0:T(128)}, u32[]{:S(2)}) copy-start(f32[128]{0:T(128)} %param.32) | copy-start | bytes 1540
  6.5 35.8 %all-gather.5.cloned.1.call-start = ((), (), s32[]{:S(2)}) async-start(), calls=%async_computation.1 | async-start | bytes 2359296 | tf_op jit(solution)/shard_map/all_gather | solution.py:386
  8.6 65.2 %all-gather.7.cloned.1.call-start = ((), (), s32[]{:S(2)}) async-start(), calls=%async_computation.2 | async-start | bytes 2359296 | tf_op jit(solution)/shard_map/all_gather | solution.py:387
  10.5 94.6 %all-gather.9.cloned.1.call-start = ((), (), s32[]{:S(2)}) async-start(), calls=%async_computation.3 | async-start | bytes 2359296 | tf_op jit(solution)/shard_map/all_gather | solution.py:388
  12.3 123.8 %all-gather.11.cloned.1.call-start = ((), (), s32[]{:S(2)}) async-start(), calls=%async_computation.4 | async-start | bytes 2359296 | tf_op jit(solution)/shard_map/all_gather | solution.py:389
  14.2 180.8 %reduce-scatter.2.cloned.1.call-start = ((), (), s32[]{:S(2)}) async-start(), calls=%async_computation.5 | async-start | bytes 1572864 | tf_op jit(solution)/shard_map/reduce_scatter | solution.py:413
  137.5 1.8 copy-start.3
  140.3 1.6 copy-start.1
  140.3 2.2 copy-start.2
  142.5 1.6 copy-start.4
  145.6 2.4 copy-start.6
  150.0 1.0 copy-start.7
  157.6 2.7 copy-start.8
  160.1 2.0 copy-start.14
  160.1 2.0 copy-start.15
  160.1 36.1 %copy-start.9 = (bf16[128,2048]{1,0:T(8,128)(2,1)S(1)}, bf16[128,2048]{1,0:T(8,128)(2,1)}, u32[]{:S(2)}) copy-start(bf16[128,2048]{1,0:T(8,128)(2,1)} %param.35) | copy-start | bytes 1572868
  160.2 36.1 %copy-start.11 = (f32[2048]{0:T(1024)S(1)}, f32[2048]{0:T(1024)}, u32[]{:S(2)}) copy-start(f32[2048]{0:T(1024)} %param.36) | copy-start | bytes 24580
  160.4 37.4 %copy-start.12 = (f32[2048]{0:T(1024)S(1)}, f32[2048]{0:T(1024)}, u32[]{:S(2)}) copy-start(f32[2048]{0:T(1024)} %param.37) | copy-start | bytes 24580
  267.7 7.4 %copy-start.18 = (bf16[1,2048,1024]{2,1,0:T(8,128)(2,1)S(1)}, bf16[1,2048,1024]{2,1,0:T(8,128)(2,1)}, u32[]{:S(2)}) copy-start(bf16[1,2048,1024]{2,1,0:T(8,128)(2,1)} %param.41) | copy-start | bytes 12582916
  272.8 2.4 copy-start.5
  309.4 78.9 %copy-start.13 = (f32[2048]{0:T(1024)S(1)}, f32[2048]{0:T(1024)}, u32[]{:S(2)}) copy-start(f32[2048]{0:T(1024)} %param.38) | copy-start | bytes 24580
Sparse Core Ops, SparseCore 0:
  8.9 33.3 all-gather.4
  44.0 29.7 all-gather.6
  75.4 29.6 all-gather.8
  106.5 29.6 all-gather.10
  162.3 32.7 reduce-scatter.1

commit v2 on v1

--- a/solution.py
+++ b/solution.py
@@ -14,51 +14,9 @@
     return values * lax.rsqrt(jnp.mean(values * values, -1, keepdims=True) + 1e-06) * gain_vec
 
 
-def attend(current, query_rows, key_rows, value_rows, first_row, query_pos, head_size):
-    run_max, run_sum, run_acc = current
-    key_count = key_rows.shape[0]
-    heads = query_rows.shape[2]
-    key_view = key_rows.reshape(key_count, 2, heads, head_size)
-    value_view = value_rows.reshape(key_count, heads, 2 * head_size)
-    key_pos = first_row + jnp.arange(key_count, dtype=jnp.int32)
-    visible = (key_pos[None, :] <= query_pos[:, None])[None, :, None, :]
-    scores = jnp.einsum(
-        "qmhd,kmhd->mqhk", query_rows, key_view, preferred_element_type=jnp.float32
-    ) * head_size ** (-0.5)
-    scores = jnp.where(visible, scores, -1e30)
-    new_max = jnp.maximum(run_max, jnp.max(scores, -1))
-    exp_terms = jnp.where(visible, jnp.exp(scores - new_max[..., None]), 0.0)
-    rescale = jnp.exp(run_max - new_max)
-    run_sum = run_sum * rescale + jnp.sum(exp_terms, -1)
-    run_acc = run_acc * rescale[..., None] + jnp.einsum(
-        "mqhk,khe->mqhe",
-        exp_terms.astype(jnp.bfloat16),
-        value_view,
-        preferred_element_type=jnp.float32,
-    )
-    return (new_max, run_sum, run_acc)
-
-
-def fresh_state(length, heads, head_size):
-    return (
-        jnp.full((2, length, heads), -1e30, jnp.float32),
-        jnp.zeros((2, length, heads), jnp.float32),
-        jnp.zeros((2, length, heads, 2 * head_size), jnp.float32),
-    )
-
-
-def finish(current, weights_two, gain_vec):
-    run_max, run_sum, run_acc = current
-    mixture = (
-        run_acc[0] / run_sum[0][..., None]
-        - weights_two[None, :, None] * run_acc[1] / run_sum[1][..., None]
-    )
-    normed = rms_norm(mixture, gain_vec)
-    return normed.reshape(normed.shape[0], -1).astype(jnp.bfloat16)
-
-
 MESH = pl.DeviceIdType.MESH
 CORES = 2
+LOG2E = 1.4426950408889634
 VMEM_BYTES = 60 * 1024 * 1024
 
 
@@ -300,6 +258,237 @@
             collective_id=2, has_side_effects=True, vmem_limit_bytes=VMEM_BYTES
         ),
     )(parts)
+
+
+def attend_kernel(
+    chips, heads_a, heads_b, query_ref, own_ref, lambda_ref, gain_a_ref, gain_b_ref, out_ref,
+    held, top, total, accum_a, accum_b, own_sem, up_sem, side_sem, recv_sem,
+):
+    chip, core, tp = place()
+    me = chip * CORES + core
+    rows = own_ref.shape[0]
+    mine = pltpu.make_async_copy(own_ref, held.at[me], own_sem)
+    mine.start()
+    barrier = pltpu.get_barrier_semaphore()
+
+    def hello(sp_to):
+        pl.semaphore_signal(barrier, inc=1, device_id={"sp": sp_to, "tp": tp}, device_id_type=MESH)
+
+    hello(chip * CORES + 1 - core)
+
+    @pl.when(chip > 0)
+    def _():
+        hello(me - CORES)
+
+    @pl.when(chip < chips - 1)
+    def _():
+        hello(me + CORES)
+
+    pl.semaphore_wait(
+        barrier, 1 + jnp.where(chip > 0, 1, 0) + jnp.where(chip < chips - 1, 1, 0)
+    )
+
+    top[...] = jnp.full_like(top, -1e30)
+    total[...] = jnp.zeros_like(total)
+    accum_a[...] = jnp.zeros_like(accum_a)
+    accum_b[...] = jnp.zeros_like(accum_b)
+    mine.wait()
+
+    def copy_up(back, index):
+        return pltpu.make_async_remote_copy(
+            src_ref=held.at[index], dst_ref=held.at[index], send_sem=up_sem.at[back],
+            recv_sem=recv_sem.at[index], device_id={"sp": me + CORES, "tp": tp}, device_id_type=MESH,
+        )
+
+    def copy_side(back, index):
+        return pltpu.make_async_remote_copy(
+            src_ref=held.at[index], dst_ref=held.at[index], send_sem=side_sem.at[back],
+            recv_sem=recv_sem.at[index], device_id={"sp": chip * CORES + 1 - core, "tp": tp},
+            device_id_type=MESH,
+        )
+
+    base_va = 2 * heads_a * DA
+    base_kb = base_va + heads_a * 2 * DA
+    base_vb = base_kb + 2 * heads_b * DB
+    base_qb = 2 * heads_a * DA
+    ahead = lax.broadcasted_iota(jnp.int32, (rows, rows), 0) - lax.broadcasted_iota(
+        jnp.int32, (rows, rows), 1
+    )
+
+    def flash(index):
+        shown = ahead + (me - index) * rows >= 0
+
+        def one(slot, query, key, value, accum, part, size):
+            scores = lax.dot_general(
+                query, key, (((1,), (1,)), ((), ())), preferred_element_type=jnp.float32
+            )
+            scores = jnp.where(shown, scores, -1e30)
+            before = top[slot]
+            after = jnp.maximum(before, jnp.max(scores, -1, keepdims=True))
+            factor = size ** (-0.5) * LOG2E
+            terms = jnp.exp2((scores - after) * factor)
+            rescale = jnp.exp2((before - after) * factor)
+            top[slot] = after
+            total[slot] = total[slot] * rescale + jnp.sum(terms, -1, keepdims=True)
+            accum[part] = accum[part] * rescale + jnp.dot(
+                terms.astype(jnp.bfloat16), value, preferred_element_type=jnp.float32
+            )
+
+        for head in range(heads_a):
+            value = held[index, :, base_va + head * 2 * DA : base_va + (head + 1) * 2 * DA]
+            for pair in range(2):
+                at = (pair * heads_a + head) * DA
+                part = pair * heads_a + head
+                one(
+                    part, query_ref[:, at : at + DA], held[index, :, at : at + DA], value,
+                    accum_a, part, DA,
+                )
+        for head in range(heads_b):
+            value = held[index, :, base_vb + head * 2 * DB : base_vb + (head + 1) * 2 * DB]
+            for pair in range(2):
+                part = pair * heads_b + head
+                at = base_qb + part * 2 * DB
+                key_at = base_kb + part // 2 * 2 * DB
+                one(
+                    2 * heads_a + part, query_ref[:, at : at + 2 * DB],
+                    held[index, :, key_at : key_at + 2 * DB], value, accum_b, part, DB,
+                )
+
+    def step(number, carry):
+        back = number // 2
+        side = number % 2
+        source = chip - back
+
+        @pl.when(source >= 0)
+        def _():
+            index = source * CORES + jnp.where(side == 0, core, 1 - core)
+
+            @pl.when(number > 0)
+            def _():
+                pltpu.make_async_copy(held.at[index], held.at[index], recv_sem.at[index]).wait()
+
+            @pl.when(side == 0)
+            def _():
+                @pl.when(chip < chips - 1)
+                def _():
+                    copy_up(back, index).start()
+
+                copy_side(back, index).start()
+
+            @pl.when(index <= me)
+            def _():
+                flash(index)
+
+        return carry
+
+    lax.fori_loop(0, 2 * chips, step, 0)
+
+    def finish(head, parts, accum, slots, lam, gain_ref, at, wide):
+        mixture = accum[parts[0]] / total[slots[0]] - lam * accum[parts[1]] / total[slots[1]]
+        out_ref[:, at : at + wide] = rms_norm(mixture, gain_ref[...]).astype(out_ref.dtype)
+
+    for head in range(heads_a):
+        parts = (head, heads_a + head)
+        finish(head, parts, accum_a, parts, lambda_ref[0:1, head : head + 1], gain_a_ref,
+               head * 2 * DA, 2 * DA)
+    for head in range(heads_b):
+        parts = (head, heads_b + head)
+        slots = (2 * heads_a + head, 2 * heads_a + heads_b + head)
+        finish(head, parts, accum_b, slots, lambda_ref[0:1, heads_a + head : heads_a + head + 1],
+               gain_b_ref, heads_a * 2 * DA + head * 2 * DB, 2 * DB)
+
+    def settle(back, carry):
+        @pl.when(chip - back >= 0)
+        def _():
+            index = (chip - back) * CORES + core
+
+            @pl.when(chip < chips - 1)
+            def _():
+                copy_up(back, index).wait_send()
+
+            copy_side(back, index).wait_send()
+
+        return carry
+
+    lax.fori_loop(0, chips, settle, 0)
+
+
+def attend_blocks(queries, own, lambdas, gain_a, gain_b, chips, heads_a, heads_b):
+    rows, width = own.shape
+    vmem = pl.BlockSpec(memory_space=pltpu.VMEM)
+    return pl.pallas_call(
+        lambda *refs: attend_kernel(chips, heads_a, heads_b, *refs),
+        name="attend_blocks",
+        out_shape=jax.ShapeDtypeStruct((rows, heads_a * 2 * DA + heads_b * 2 * DB), jnp.bfloat16),
+        in_specs=[vmem, pl.BlockSpec(memory_space=pl.ANY), vmem, vmem, vmem],
+        out_specs=vmem,
+        scratch_shapes=[
+            pltpu.VMEM((chips * CORES, rows, width), own.dtype),
+            pltpu.VMEM((2 * (heads_a + heads_b), rows, 1), jnp.float32),
+            pltpu.VMEM((2 * (heads_a + heads_b), rows, 1), jnp.float32),
+            pltpu.VMEM((2 * heads_a, rows, 2 * DA), jnp.float32),
+            pltpu.VMEM((2 * heads_b, rows, 2 * DB), jnp.float32),
+            pltpu.SemaphoreType.DMA,
+            pltpu.SemaphoreType.DMA((chips,)),
+            pltpu.SemaphoreType.DMA((chips,)),
+            pltpu.SemaphoreType.DMA((chips * CORES,)),
+        ],
+        compiler_params=pltpu.CompilerParams(
+            collective_id=3, has_side_effects=True, vmem_limit_bytes=VMEM_BYTES
+        ),
+    )(queries, own, lambdas, gain_a, gain_b)
+
+
+def share_kernel(tps, part_ref, out_ref, arrived, send_sem, recv_sem):
+    tp = lax.axis_index("tp")
+    barrier = pltpu.get_barrier_semaphore()
+    for step in range(1, tps):
+        pl.semaphore_signal(barrier, inc=1, device_id={"tp": (tp + step) % tps}, device_id_type=MESH)
+    pl.semaphore_wait(barrier, tps - 1)
+    started = []
+    for step in range(1, tps):
+        other = (tp + step) % tps
+        copy = pltpu.make_async_remote_copy(
+            src_ref=part_ref.at[other], dst_ref=arrived.at[step - 1], send_sem=send_sem.at[step - 1],
+            recv_sem=recv_sem.at[step - 1], device_id={"tp": other}, device_id_type=MESH,
+        )
+        copy.start()
+        started.append(copy)
+    rows = out_ref.shape[0]
+    chunk = min(rows, 16)
+    for step in range(1, tps):
+        started[step - 1].wait()
+
+        @pl.loop(0, rows // chunk)
+        def _(part):
+            span = pl.ds(pl.multiple_of(part * chunk, chunk), chunk)
+            first = part_ref[tp, span, :].astype(jnp.float32) if step == 1 else out_ref[span, :]
+            out_ref[span, :] = first + arrived[step - 1, span, :].astype(jnp.float32)
+
+
+def share_rows(parts, tps):
+    _, rows, width = parts.shape
+    vmem = pl.BlockSpec(memory_space=pltpu.VMEM)
+    return pl.pallas_call(
+        lambda *refs: share_kernel(tps, *refs),
+        name="share_rows",
+        out_shape=jax.ShapeDtypeStruct((rows, width), jnp.float32),
+        in_specs=[vmem],
+        out_specs=vmem,
+        scratch_shapes=[
+            pltpu.VMEM((tps - 1, rows, width), parts.dtype),
+            pltpu.SemaphoreType.DMA((tps - 1,)),
+            pltpu.SemaphoreType.DMA((tps - 1,)),
+        ],
+        compiler_params=pltpu.CompilerParams(collective_id=4, has_side_effects=True),
+    )(parts)
+
+
+def spread_pairs(queries, heads):
+    rows = queries.shape[0]
+    pairs = queries.reshape(rows, 2 * heads // 2, 1, 2, DB)
+    keep = jnp.eye(2, dtype=queries.dtype).reshape(1, 1, 2, 2, 1)
+    return (pairs * keep).reshape(rows, 2 * heads * 2 * DB)
 
 
 def expert_parts(gathered, expert, experts, capacity, width, weights):
@@ -365,68 +554,34 @@
     seq_slot = lax.axis_index("sp")
     lambda_a = lax.dynamic_slice_in_dim(lambdas, head_slot * heads_a, heads_a)
     lambda_b = lax.dynamic_slice_in_dim(lambdas, HA + head_slot * heads_b, heads_b)
-    groups = [
-        (
-            queries_a.reshape(length, 2, heads_a, DA),
-            queries_b.reshape(length, 2, heads_b, DB),
-            seq_slot * length + jnp.arange(length, dtype=jnp.int32),
-            seq_slot * length + length - 1,
-        )
-    ]
-    initial = tuple(
-        (
-            (
-                fresh_state(group[2].shape[0], heads_a, DA),
-                fresh_state(group[2].shape[0], heads_b, DB),
-            )
-            for group in groups
-        )
-    )
-    pieces = (
-        lax.all_gather(keys_a, "sp", axis=0, tiled=True),
-        lax.all_gather(values_a, "sp", axis=0, tiled=True),
-        lax.all_gather(keys_b, "sp", axis=0, tiled=True),
-        lax.all_gather(values_b, "sp", axis=0, tiled=True),
-    )
-    key_count = pieces[0].shape[0]
-    span_rows = 1024
-
-    def one_span(span_index, carried):
-        offset = span_index * span_rows
-        parts = tuple(
-            (lax.dynamic_slice_in_dim(piece_part, offset, span_rows, 0) for piece_part in pieces)
-        )
-        group_qa, group_qb, group_pos, group_last = groups[0]
-
-        def compute(inner, group_qa=group_qa, group_qb=group_qb, group_pos=group_pos):
-            return (
-                attend(inner[0], group_qa, parts[0], parts[1], offset, group_pos, DA),
-                attend(inner[1], group_qb, parts[2], parts[3], offset, group_pos, DB),
-            )
-
-        updated = [lax.cond(offset <= group_last, compute, lambda inner: inner, carried[0])]
-        return tuple(updated)
-
-    final_state = lax.fori_loop(0, key_count // span_rows, one_span, initial)
-    heads_out_a = finish(final_state[0][0], lambda_a, head_gain_a)
-    heads_out_b = finish(final_state[0][1], lambda_b, head_gain_b)
-    mixed_rows = lax.psum_scatter(
-        (
-            jnp.dot(heads_out_a, out_a, preferred_element_type=jnp.float32)
-            + jnp.dot(heads_out_b, out_b, preferred_element_type=jnp.float32)
-        ).astype(jnp.bfloat16),
-        "tp",
-        scatter_dimension=0,
-        tiled=True,
-    ).astype(jnp.float32)
+    experts, tps = lax.axis_size("sp"), lax.axis_size("tp")
+    chips = experts // CORES
+    own = jnp.concatenate(
+        [keys_a.reshape(length, -1), values_a, keys_b.reshape(length, -1), values_b], 1
+    )
+    queries = jnp.concatenate([queries_a.reshape(length, -1), spread_pairs(queries_b, heads_b)], 1)
+    heads_out = attend_blocks(
+        queries,
+        own,
+        jnp.concatenate([lambda_a, lambda_b])[None],
+        head_gain_a[None],
+        head_gain_b[None],
+        chips,
+        heads_a,
+        heads_b,
+    )
+    cut = heads_a * 2 * DA
+    mixed = (
+        jnp.dot(heads_out[:, :cut], out_a, preferred_element_type=jnp.float32)
+        + jnp.dot(heads_out[:, cut:], out_b, preferred_element_type=jnp.float32)
+    ).astype(jnp.bfloat16)
+    mixed_rows = share_rows(mixed.reshape(tps, length // tps, -1), tps)
     after_mix = (residual.astype(jnp.float32) + rms_norm(mixed_rows, gain_mix)).astype(jnp.bfloat16)
     normed = rms_norm(after_mix.astype(jnp.float32), gain_pre).astype(jnp.bfloat16)
-    experts = lax.axis_size("sp")
     sub_rows = residual.shape[0]
     top_count = routes.shape[1]
     capacity = min(sub_rows, (5 * sub_rows * top_count + 4 * experts - 1) // (4 * experts))
     width = residual.shape[1]
-    chips, tps = experts // CORES, lax.axis_size("tp")
     extra = -(-experts // 128) * 128
     shares = jnp.sum(
         jnp.where(

time: 398 us -> 308 us (0.77)
  waiting for transfers between devices: 151 us -> 0 us
  Pallas kernels: 145 us -> 240 us
  local copies, waits for them, and re-layouts: 24.7 us -> 10.6 us
  between operations: 13.4 us -> 0.19 us
    all_gather x4 -> x0, waiting for transfers between devices: 119 us -> none  [the longest x1 31.4 us: per_device(): lax.all_gather(values_a, 'sp', axis=0, tiled=True)]
    pallas_call x1, Pallas kernels: 67.3 us -> 121 us  [gather_rows(): pl.pallas_call(lambda *refs: gather_kernel(chips, tps, *refs), name='gath...]
    pallas_call x0 -> x2, Pallas kernels: none -> 43.1 us  [the longest x1 27.9 us: attend_blocks(): pl.pallas_call(lambda *refs: attend_kernel(chips, heads_a, heads_b, *refs...]
    reduce_scatter x1 -> x0, waiting for transfers between devices: 32.7 us -> none  [per_device(): lax.psum_scatter((jnp.dot(heads_out_a, out_a, preferred_element_type=jnp....]
    unnamed x39 -> x20, local copies, waits for them, and re-layouts: 12.7 us -> 7.15 us
    convert_element_type x4 -> x1, other arithmetic: 5.24 us -> 0.01 us  [spread_pairs(): keep = jnp.eye(2, dtype=queries.dtype).reshape(1, 1, 2, 2, 1)]
    dot_general x6 -> x2, matrix products: 8.28 us -> 4.55 us  [the longest x1 2.75 us: per_device(): jnp.dot(heads_out[:, cut:], out_b, preferred_element_type=jnp.float32)]
  transfers between devices with their start and end apart: 5 -> 0, of which waited for: 5 -> 0; matrix products, arithmetic and copies ran while one was open for 2% -> 0% of each run, Pallas kernels for 0% -> 0%
where the time goes in v2:
time: 308 us; the launch traced here: 307 us
  Pallas kernels  240 us (78%)
  matrix products  44 us (14%)
  other arithmetic  12.4 us (4%)
  local copies, waits for them, and re-layouts  10.6 us (3%)
    pallas_call x1, Pallas kernels, gather_rows(): pl.pallas_call(lambda *refs: gather_kernel(chips, tps, *refs), name='gath...  121 us
    pallas_call x1, Pallas kernels, scatter_rows(): pl.pallas_call(lambda *refs: scatter_kernel(chips, tps, *refs), name='sca...  76.2 us
    pallas_call x1, Pallas kernels, attend_blocks(): pl.pallas_call(lambda *refs: attend_kernel(chips, heads_a, heads_b, *refs...  27.9 us
    dot_general x1, matrix products, expert_parts(): jnp.dot(hidden, down, preferred_element_type=jnp.float32)  18.7 us
    pallas_call x1, Pallas kernels, share_rows(): pl.pallas_call(lambda *refs: share_kernel(tps, *refs), name='share_rows',...  15.2 us
    dot_general x1, matrix products, expert_parts(): jnp.einsum('bct,bcd->btd', back, outs.reshape(blocks, capacity, width), p...  8.19 us
    dot_general x1, matrix products, expert_parts(): gate_pre = jnp.dot(rows_in, gate, preferred_element_type=jnp.float32)  7.35 us
    unnamed x20, local copies, waits for them, and re-layouts  7.15 us

profile of v2, /device:TPU:0, one launch (start us, length us, event | category | flops | bytes accessed | tf_op | source)
XLA Modules:
  0.0 307.2 jit_solution(4556425677709161514)
XLA Ops:
  0.0 0.0 copy-start
  0.0 0.9 dynamic_slice.10
  0.9 0.7 dynamic_slice.9
  1.6 0.6 maximum_bitcast_fusion.refs_2_
  2.2 0.1 mul.100
  2.3 0.1 mul.101
  2.4 0.9 select_reduce_fusion
  3.3 1.0 copy.29
  4.2 1.7 copy.30
  5.9 1.1 copy.27
  7.1 0.2 copy.28
  7.4 0.9 pad_maximum_fusion.1.refs_0_
  8.3 1.0 copy.31
  9.3 2.2 pad_maximum_fusion.refs_1_
  11.5 27.9 %attend_blocks.1 = bf16[256,1024]{1,0:T(8,128)(2,1)} custom-call(bf16[256,1536]{1,0:T(8,128)(2,1)} %pad_maximum_fusion.1.refs_0_, bf16[256,2048]{1,0:T(8,128)(2,1)} %pad_maximum_fusion.refs_1_, f32[1,6]{1,0:T(1,128)} %maximum_bitcast_fusion.refs_2_, f32[1,256]{1,0:T(1,128)} %bitcast.44, f32[1,128]{1,0:T(1,128)} %bitcast.45), custom_call_target="tpu_custom_call" | custom-call | tf_op jit(solution)/shard_map/attend_blocks/pallas_call | solution.py:419
  39.4 0.0 copy-done
  39.4 0.0 copy-start.2
  39.5 1.8 fusion.29
  41.3 0.0 copy-done.2
  41.3 0.0 copy-start.3
  41.3 0.0 copy-start.4
  41.3 0.0 copy-start.5
  41.3 2.7 fusion.15
  44.1 15.2 %share_rows.1 = f32[128,2048]{1,0:T(8,128)} custom-call(bf16[2,128,2048]{2,1,0:T(8,128)(2,1)} %bitcast.35), custom_call_target="tpu_custom_call" | custom-call | tf_op jit(solution)/shard_map/share_rows/pallas_call | solution.py:472
  59.2 1.4 multiply_reduce_fusion.1
  60.6 0.0 copy-done.3
  60.6 0.0 copy-done.4
  60.6 1.6 fusion.16
  62.2 0.0 copy-done.5
  62.2 0.2 fusion.18
  62.4 0.9 pad_maximum_fusion.2.refs_0_
  63.3 120.6 %gather_rows.1 = bf16[16,128,2176]{2,1,0:T(8,128)(2,1)} custom-call(bf16[128,2176]{1,0:T(8,128)(2,1)} %pad_maximum_fusion.2.refs_0_), custom_call_target="tpu_custom_call" | custom-call | tf_op jit(solution)/shard_map/gather_rows/pallas_call | solution.py:107
  184.0 1.1 slice.14
  185.1 0.4 dynamic-slice_reduce_fusion
  185.5 0.1 convolution_convert_fusion.2
  185.6 0.0 copy-start.7
  185.6 5.1 %fusion.6 = bf16[16,80,2048]{2,1,0:T(8,128)(2,1)S(1)} fusion(bf16[16,128,2176]{2,1,0:T(8,128)(2,1)} %gather_rows.1, s32[16,128]{1,0:T(8,128)S(1)} %convolution_convert_fusion.2, pred[16,128]{1,0:T(8,128)(4,1)S(1)} %broadcast_compare_fusion), kind=kOutput, calls=%fused_computation.9 | convolution fusion | flops 674037760 | bytes 13641728 | tf_op jit(solution)/shard_map/bct,btd->bcd/dot_general | solution.py:506
  190.7 0.0 copy-start.1
  190.7 2.4 copy-done.1
  193.1 0.0 copy-done.7
  193.1 7.3 %fusion.4 = f32[1280,1024]{1,0:T(8,128)} fusion(bf16[1280,2048]{1,0:T(8,128)(2,1)S(1)} %bitcast.32, bf16[1,2048,1024]{2,1,0:T(8,128)(2,1)S(1)} %copy-done.7), kind=kOutput, calls=%fused_computation.7 | convolution fusion | flops 5368709120 | bytes 14680064 | tf_op jit(solution)/shard_map/dot_general | solution.py:513
  200.4 18.7 %convolution_convert_fusion = bf16[1280,2048]{1,0:T(8,128)(2,1)} fusion(bf16[1,1024,2048]{2,1,0:T(8,128)(2,1)} %param.39, f32[1280,1024]{1,0:T(8,128)} %fusion.4, bf16[1280,2048]{1,0:T(8,128)(2,1)} %bitcast.33, bf16[1,2048,1024]{2,1,0:T(8,128)(2,1)} %param.38), kind=kOutput, calls=%fused_computation.2 | convolution fusion | flops 10753146880 | bytes 24117248 | tf_op jit(solution)/shard_map/dot_general | solution.py:518
  219.1 8.2 %convolution_convert_fusion.1.refs_0_ = bf16[16,128,2048]{2,1,0:T(8,128)(2,1)} fusion(bf16[16,80,2048]{2,1,0:T(8,128)(2,1)} %bitcast.34, s32[16,128]{1,0:T(8,128)S(1)} %convolution_convert_fusion.2, pred[16,128]{1,0:T(8,128)(4,1)S(1)} %broadcast_compare_fusion, bf16[16,128]{1,0:T(8,128)(2,1)S(1)} %dynamic-slice_reduce_fusion), kind=kOutput, calls=%fused_computation.3 | convolution fusion | flops 675774464 | bytes 13645824 | tf_op jit(solution)/shard_map/bct,bcd->btd/dot_general | solution.py:520
  227.3 0.0 copy-start.6
  227.3 76.2 %scatter_rows.1 = f32[128,2048]{1,0:T(8,128)} custom-call(bf16[16,128,2048]{2,1,0:T(8,128)(2,1)} %convolution_convert_fusion.1.refs_0_), custom_call_target="tpu_custom_call" | custom-call | tf_op jit(solution)/shard_map/scatter_rows/pallas_call | solution.py:240
  303.5 1.4 multiply_reduce_fusion
  304.9 0.0 copy-done.6
  304.9 2.2 fusion.19
  (7 shorter events, 0.1 us)
Async XLA Ops:
  0.0 39.4 %copy-start = (bf16[512,2048]{1,0:T(8,128)(2,1)S(1)}, bf16[512,2048]{1,0:T(8,128)(2,1)}, u32[]{:S(2)}) copy-start(bf16[512,2048]{1,0:T(8,128)(2,1)} %param.29) | copy-start | bytes 6291460
  39.4 1.8 copy-start.2
  41.3 19.3 %copy-start.3 = (bf16[128,2048]{1,0:T(8,128)(2,1)S(1)}, bf16[128,2048]{1,0:T(8,128)(2,1)}, u32[]{:S(2)}) copy-start(bf16[128,2048]{1,0:T(8,128)(2,1)} %param.31) | copy-start | bytes 1572868
  41.3 19.3 %copy-start.4 = (f32[2048]{0:T(1024)S(1)}, f32[2048]{0:T(1024)}, u32[]{:S(2)}) copy-start(f32[2048]{0:T(1024)} %param.32) | copy-start | bytes 24580
  41.3 20.9 %copy-start.5 = (f32[2048]{0:T(1024)S(1)}, f32[2048]{0:T(1024)}, u32[]{:S(2)}) copy-start(f32[2048]{0:T(1024)} %param.33) | copy-start | bytes 24580
  185.6 7.4 %copy-start.7 = (bf16[1,2048,1024]{2,1,0:T(8,128)(2,1)S(1)}, bf16[1,2048,1024]{2,1,0:T(8,128)(2,1)}, u32[]{:S(2)}) copy-start(bf16[1,2048,1024]{2,1,0:T(8,128)(2,1)} %param.37) | copy-start | bytes 12582916
  190.7 2.4 copy-start.1
  227.3 77.6 %copy-start.6 = (f32[2048]{0:T(1024)S(1)}, f32[2048]{0:T(1024)}, u32[]{:S(2)}) copy-start(f32[2048]{0:T(1024)} %param.34) | copy-start | bytes 24580

commit v3 on v2

--- a/solution.py
+++ b/solution.py
@@ -16,6 +16,7 @@
 
 MESH = pl.DeviceIdType.MESH
 CORES = 2
+PIECES = 2
 LOG2E = 1.4426950408889634
 VMEM_BYTES = 60 * 1024 * 1024
 
@@ -51,8 +52,8 @@
     greet(chips, tps)
     started = []
 
-    def block(chip_of, core_of, tp_of):
-        return (chip_of * CORES + core_of) * tps + tp_of
+    def block(chip_of, core_of, tp_of, piece):
+        return ((chip_of * CORES + core_of) * tps + tp_of) * PIECES + piece
 
     def send(source, index, sp_to, tp_to):
         copy = pltpu.make_async_remote_copy(
@@ -69,45 +70,53 @@
     def arrived(index):
         pltpu.make_async_copy(all_ref.at[index], all_ref.at[index], recv_sem.at[index]).wait()
 
-    own = block(chip, core, tp)
-    for step in range(1, chips):
-        send(own_ref, own, (chip + step) % chips * CORES + core, tp)
-    for step in range(1, tps):
-        send(own_ref, own, chip * CORES + core, (tp + step) % tps)
-    send(own_ref, own, chip * CORES + 1 - core, tp)
-    mine = pltpu.make_async_copy(own_ref, all_ref.at[own], own_sem)
+    for piece in range(PIECES):
+        own = block(chip, core, tp, piece)
+        for step in range(1, tps):
+            send(own_ref.at[piece], own, chip * CORES + core, (tp + step) % tps)
+        for step in range(1, chips):
+            send(own_ref.at[piece], own, (chip + step) % chips * CORES + core, tp)
+        send(own_ref.at[piece], own, chip * CORES + 1 - core, tp)
+    mine = pltpu.make_async_copy(
+        own_ref, all_ref.at[pl.ds(block(chip, core, tp, 0), PIECES)], own_sem
+    )
     mine.start()
 
-    def from_tp(chip_of):
+    def from_tp(chip_of, piece):
         for step in range(1, tps):
-            index = block(chip_of, core, (tp + step) % tps)
+            index = block(chip_of, core, (tp + step) % tps, piece)
             arrived(index)
             send(all_ref.at[index], index, chip * CORES + 1 - core, tp)
 
-    for step in range(1, chips):
-        chip_of = (chip - step + chips) % chips
-        index = block(chip_of, core, tp)
-        arrived(index)
-        for tp_step in range(1, tps):
-            send(all_ref.at[index], index, chip * CORES + core, (tp + tp_step) % tps)
-        send(all_ref.at[index], index, chip * CORES + 1 - core, tp)
-        from_tp((chip - step + 1 + chips) % chips)
-    from_tp((chip + 1) % chips)
-    for step in range(chips):
+    order = [(step, piece) for step in range(chips) for piece in range(PIECES)]
+    for place_in, (step, piece) in enumerate(order):
+        if step > 0:
+            index = block((chip - step + chips) % chips, core, tp, piece)
+            arrived(index)
+            for tp_step in range(1, tps):
+                send(all_ref.at[index], index, chip * CORES + core, (tp + tp_step) % tps)
+            send(all_ref.at[index], index, chip * CORES + 1 - core, tp)
+            done, done_piece = order[place_in - PIECES]
+            from_tp((chip - done + chips) % chips, done_piece)
+    for piece in range(PIECES):
+        from_tp((chip + 1) % chips, piece)
+    for step, piece in order:
         for tp_of in range(tps):
-            arrived(block((chip - step + chips) % chips, 1 - core, (tp + tp_of) % tps))
+            arrived(block((chip - step + chips) % chips, 1 - core, (tp + tp_of) % tps, piece))
     mine.wait()
     for copy in started:
         copy.wait_send()
 
 
 def gather_rows(own, chips, tps):
-    blocks = chips * CORES * tps
-    sends = chips - 1 + tps - 1 + 1 + (chips - 1) * tps + chips * (tps - 1)
+    blocks = chips * CORES * tps * PIECES
+    sends = (chips - 1 + tps - 1 + 1 + (chips - 1) * tps + chips * (tps - 1)) * PIECES
+    rows, width = own.shape
+    own = own.reshape(PIECES, rows // PIECES, width)
     return pl.pallas_call(
         lambda *refs: gather_kernel(chips, tps, *refs),
         name="gather_rows",
-        out_shape=jax.ShapeDtypeStruct((blocks,) + own.shape, own.dtype),
+        out_shape=jax.ShapeDtypeStruct((blocks,) + own.shape[1:], own.dtype),
         in_specs=[pl.BlockSpec(memory_space=pl.ANY)],
         out_specs=pl.BlockSpec(memory_space=pl.ANY),
         scratch_shapes=[
@@ -116,7 +125,7 @@
             pltpu.SemaphoreType.DMA,
         ],
         compiler_params=pltpu.CompilerParams(collective_id=1, has_side_effects=True),
-    )(own)
+    )(own).reshape(-1, rows, width)
 
 
 def add_rows(target, index, source, source_index):
@@ -138,13 +147,14 @@
     chip, core, tp = place()
     load = []
     started = []
-    for step in range(chips):
+    order = [(step, piece) for step in range(chips) for piece in range(PIECES)]
+    for step, piece in order:
         for tp_step in range(tps):
             chip_of, tp_of = (chip + 1 + step) % chips, (tp + 1 + tp_step) % tps
             copy = pltpu.make_async_copy(
-                part_ref.at[(chip_of * CORES + core) * tps + tp_of],
-                acc.at[chip_of * tps + tp_of],
-                load_sem.at[step * tps + tp_step],
+                part_ref.at[((chip_of * CORES + core) * tps + tp_of) * PIECES + piece],
+                acc.at[(chip_of * tps + tp_of) * PIECES + piece],
+                load_sem.at[len(load)],
             )
             copy.start()
             load.append(copy)
@@ -165,69 +175,63 @@
     def arrived(target, index, sem):
         pltpu.make_async_copy(target.at[index], target.at[index], sem).wait()
 
-    for step in range(chips):
+    for step, piece in order:
         chip_of = (chip + 1 + step) % chips
         for tp_step in range(tps):
             tp_of = (tp + 1 + tp_step) % tps
-            index = chip_of * tps + tp_of
+            index = (chip_of * tps + tp_of) * PIECES + piece
             send(
-                part_ref.at[(chip_of * CORES + 1 - core) * tps + tp_of],
+                part_ref.at[((chip_of * CORES + 1 - core) * tps + tp_of) * PIECES + piece],
                 core_in.at[index],
                 core_sem.at[index],
                 chip * CORES + 1 - core,
                 tp,
             )
 
-    def chip_stage(step):
+    def chip_stage(step, piece):
         chip_of = (chip + 1 + step) % chips
+        kept = (chip_of * tps + tp) * PIECES + piece
         for tp_step in range(1, tps):
-            source = (tp + tp_step) % tps
-            index = chip_of * tps + source
+            index = (chip_of * tps + (tp + tp_step) % tps) * PIECES + piece
             arrived(tp_in, index, tp_sem.at[index])
-            add_rows(acc, chip_of * tps + tp, tp_in, index)
+            add_rows(acc, kept, tp_in, index)
         if step < chips - 1:
-            send(
-                acc.at[chip_of * tps + tp],
-                chip_in.at[chip],
-                chip_sem.at[chip],
-                chip_of * CORES + core,
-                tp,
-            )
-
-    for step in range(chips):
+            slot = chip * PIECES + piece
+            send(acc.at[kept], chip_in.at[slot], chip_sem.at[slot], chip_of * CORES + core, tp)
+
+    for number, (step, piece) in enumerate(order):
         chip_of = (chip + 1 + step) % chips
         for tp_step in range(tps):
             tp_of = (tp + 1 + tp_step) % tps
-            index = chip_of * tps + tp_of
-            load[step * tps + tp_step].wait()
+            index = (chip_of * tps + tp_of) * PIECES + piece
+            load[number * tps + tp_step].wait()
             arrived(core_in, index, core_sem.at[index])
             add_rows(acc, index, core_in, index)
             if tp_step < tps - 1:
+                slot = (chip_of * tps + tp) * PIECES + piece
                 send(
-                    acc.at[index],
-                    tp_in.at[chip_of * tps + tp],
-                    tp_sem.at[chip_of * tps + tp],
-                    chip * CORES + core,
-                    tp_of,
+                    acc.at[index], tp_in.at[slot], tp_sem.at[slot], chip * CORES + core, tp_of
                 )
-        if step > 0:
-            chip_stage(step - 1)
-    chip_stage(chips - 1)
+        if number > 0:
+            chip_stage(*order[number - 1])
+    chip_stage(*order[-1])
+    rows = out_ref.shape[1]
+    chunk = min(rows, 16)
     for step in range(1, chips):
-        source = (chip - step + chips) % chips
-        arrived(chip_in, source, chip_sem.at[source])
-        if step < chips - 1:
-            add_rows(acc, chip * tps + tp, chip_in, source)
-    last = (chip + 1) % chips
-    rows = out_ref.shape[0]
-    chunk = min(rows, 16)
-
-    @pl.loop(0, rows // chunk)
-    def _(part):
-        span = pl.ds(pl.multiple_of(part * chunk, chunk), chunk)
-        out_ref[span, :] = acc[chip * tps + tp, span, :].astype(jnp.float32) + chip_in[
-            last, span, :
-        ].astype(jnp.float32)
+        for piece in range(PIECES):
+            source = (chip - step + chips) % chips * PIECES + piece
+            kept = (chip * tps + tp) * PIECES + piece
+            arrived(chip_in, source, chip_sem.at[source])
+            if step < chips - 1:
+                add_rows(acc, kept, chip_in, source)
+            else:
+
+                @pl.loop(0, rows // chunk)
+                def _(part):
+                    span = pl.ds(pl.multiple_of(part * chunk, chunk), chunk)
+                    out_ref[piece, span, :] = acc[kept, span, :].astype(jnp.float32) + chip_in[
+                        source, span, :
+                    ].astype(jnp.float32)
 
     for copy in started:
         copy.wait_send()
@@ -235,29 +239,30 @@
 
 def scatter_rows(parts, chips, tps):
     blocks, rows, width = parts.shape
-    half = chips * tps
-    sends = half + chips * (tps - 1) + chips - 1
+    half = chips * tps * PIECES
+    sends = half + (chips * (tps - 1) + chips - 1) * PIECES
+    rows = rows // PIECES
     return pl.pallas_call(
         lambda *refs: scatter_kernel(chips, tps, *refs),
         name="scatter_rows",
-        out_shape=jax.ShapeDtypeStruct((rows, width), jnp.float32),
+        out_shape=jax.ShapeDtypeStruct((PIECES, rows, width), jnp.float32),
         in_specs=[pl.BlockSpec(memory_space=pl.ANY)],
         out_specs=pl.BlockSpec(memory_space=pltpu.VMEM),
         scratch_shapes=[
             pltpu.VMEM((half, rows, width), parts.dtype),
             pltpu.VMEM((half, rows, width), parts.dtype),
             pltpu.VMEM((half, rows, width), parts.dtype),
-            pltpu.VMEM((chips, rows, width), parts.dtype),
+            pltpu.VMEM((chips * PIECES, rows, width), parts.dtype),
             pltpu.SemaphoreType.DMA((half,)),
             pltpu.SemaphoreType.DMA((sends,)),
             pltpu.SemaphoreType.DMA((half,)),
             pltpu.SemaphoreType.DMA((half,)),
-            pltpu.SemaphoreType.DMA((chips,)),
+            pltpu.SemaphoreType.DMA((chips * PIECES,)),
         ],
         compiler_params=pltpu.CompilerParams(
             collective_id=2, has_side_effects=True, vmem_limit_bytes=VMEM_BYTES
         ),
-    )(parts)
+    )(parts.reshape(-1, rows, width)).reshape(PIECES * rows, width)
 
 
 def attend_kernel(

time: 308 us -> 301 us (0.977)
  Pallas kernels: 240 us -> 233 us
    pallas_call x1, Pallas kernels: 76.2 us -> 69.5 us  [scatter_rows(): pl.pallas_call(lambda *refs: scatter_kernel(chips, tps, *refs), name='sca...]
where the time goes in v3:
time: 301 us; the launch traced here: 300 us
  Pallas kernels  233 us (77%)
  matrix products  44 us (15%)
  other arithmetic  12.4 us (4%)
  local copies, waits for them, and re-layouts  10.7 us (4%)
    pallas_call x1, Pallas kernels, gather_rows(): pl.pallas_call(lambda *refs: gather_kernel(chips, tps, *refs), name='gath...  121 us
    pallas_call x1, Pallas kernels, scatter_rows(): pl.pallas_call(lambda *refs: scatter_kernel(chips, tps, *refs), name='sca...  69.5 us
    pallas_call x1, Pallas kernels, attend_blocks(): pl.pallas_call(lambda *refs: attend_kernel(chips, heads_a, heads_b, *refs...  27.9 us
    dot_general x1, matrix products, expert_parts(): jnp.dot(hidden, down, preferred_element_type=jnp.float32)  18.7 us
    pallas_call x1, Pallas kernels, share_rows(): pl.pallas_call(lambda *refs: share_kernel(tps, *refs), name='share_rows',...  15.2 us
    dot_general x1, matrix products, expert_parts(): jnp.einsum('bct,bcd->btd', back, outs.reshape(blocks, capacity, width), p...  8.19 us
    dot_general x1, matrix products, expert_parts(): gate_pre = jnp.dot(rows_in, gate, preferred_element_type=jnp.float32)  7.35 us
    unnamed x20, local copies, waits for them, and re-layouts  7.15 us

profile of v3, /device:TPU:0, one launch (start us, length us, event | category | flops | bytes accessed | tf_op | source)
XLA Modules:
  0.0 300.4 jit_solution(15533948815563409269)
XLA Ops:
  0.0 0.0 copy-start
  0.0 0.9 dynamic_slice.10
  0.9 0.7 dynamic_slice.9
  1.6 0.6 maximum_bitcast_fusion.refs_2_
  2.2 0.1 mul.101
  2.3 0.1 mul.102
  2.4 0.9 select_reduce_fusion
  3.3 1.0 copy.29
  4.2 1.7 copy.30
  5.9 1.1 copy.27
  7.1 0.2 copy.28
  7.4 0.9 pad_maximum_fusion.1.refs_0_
  8.3 1.0 copy.31
  9.3 2.2 pad_maximum_fusion.refs_1_
  11.5 27.9 %attend_blocks.1 = bf16[256,1024]{1,0:T(8,128)(2,1)} custom-call(bf16[256,1536]{1,0:T(8,128)(2,1)} %pad_maximum_fusion.1.refs_0_, bf16[256,2048]{1,0:T(8,128)(2,1)} %pad_maximum_fusion.refs_1_, f32[1,6]{1,0:T(1,128)} %maximum_bitcast_fusion.refs_2_, f32[1,256]{1,0:T(1,128)} %bitcast.57, f32[1,128]{1,0:T(1,128)} %bitcast.58), custom_call_target="tpu_custom_call" | custom-call | tf_op jit(solution)/shard_map/attend_blocks/pallas_call | solution.py:424
  39.4 0.0 copy-done
  39.4 0.0 copy-start.2
  39.5 1.8 fusion.30
  41.3 0.0 copy-done.2
  41.3 0.0 copy-start.3
  41.3 0.0 copy-start.4
  41.3 0.0 copy-start.5
  41.3 2.7 fusion.15
  44.1 15.2 %share_rows.1 = f32[128,2048]{1,0:T(8,128)} custom-call(bf16[2,128,2048]{2,1,0:T(8,128)(2,1)} %bitcast.47), custom_call_target="tpu_custom_call" | custom-call | tf_op jit(solution)/shard_map/share_rows/pallas_call | solution.py:477
  59.2 1.4 multiply_reduce_fusion.1
  60.6 0.0 copy-done.3
  60.6 0.0 copy-done.4
  60.6 1.6 fusion.16
  62.2 0.0 copy-done.5
  62.2 0.2 fusion.18
  62.4 0.9 pad_maximum_fusion.2
  63.3 120.6 %gather_rows.1 = bf16[32,64,2176]{2,1,0:T(8,128)(2,1)} custom-call(bf16[2,64,2176]{2,1,0:T(8,128)(2,1)} %bitcast.48), custom_call_target="tpu_custom_call" | custom-call | tf_op jit(solution)/shard_map/gather_rows/pallas_call | solution.py:116
  183.9 1.1 slice.16
  185.0 0.4 dynamic-slice_reduce_fusion
  185.4 0.1 convolution_convert_fusion.2
  185.5 0.0 copy-start.7
  185.5 5.1 %fusion.6 = bf16[16,80,2048]{2,1,0:T(8,128)(2,1)S(1)} fusion(bf16[16,128,2176]{2,1,0:T(8,128)(2,1)} %bitcast.42, s32[16,128]{1,0:T(8,128)S(1)} %convolution_convert_fusion.2, pred[16,128]{1,0:T(8,128)(4,1)S(1)} %broadcast_compare_fusion), kind=kOutput, calls=%fused_computation.9 | convolution fusion | flops 674037760 | bytes 13641728 | tf_op jit(solution)/shard_map/bct,btd->bcd/dot_general | solution.py:511
  190.6 0.0 copy-start.1
  190.6 2.4 copy-done.1
  193.0 0.0 copy-done.7
  193.0 7.3 %fusion.4 = f32[1280,1024]{1,0:T(8,128)} fusion(bf16[1280,2048]{1,0:T(8,128)(2,1)S(1)} %bitcast.44, bf16[1,2048,1024]{2,1,0:T(8,128)(2,1)S(1)} %copy-done.7), kind=kOutput, calls=%fused_computation.7 | convolution fusion | flops 5368709120 | bytes 14680064 | tf_op jit(solution)/shard_map/dot_general | solution.py:518
  200.3 18.7 %convolution_convert_fusion = bf16[1280,2048]{1,0:T(8,128)(2,1)} fusion(bf16[1,1024,2048]{2,1,0:T(8,128)(2,1)} %param.39, f32[1280,1024]{1,0:T(8,128)} %fusion.4, bf16[1280,2048]{1,0:T(8,128)(2,1)} %bitcast.45, bf16[1,2048,1024]{2,1,0:T(8,128)(2,1)} %param.38), kind=kOutput, calls=%fused_computation.2 | convolution fusion | flops 10753146880 | bytes 24117248 | tf_op jit(solution)/shard_map/dot_general | solution.py:523
  219.0 8.2 %convolution_convert_fusion.1 = bf16[16,128,2048]{2,1,0:T(8,128)(2,1)} fusion(bf16[16,80,2048]{2,1,0:T(8,128)(2,1)} %bitcast.46, s32[16,128]{1,0:T(8,128)S(1)} %convolution_convert_fusion.2, pred[16,128]{1,0:T(8,128)(4,1)S(1)} %broadcast_compare_fusion, bf16[16,128]{1,0:T(8,128)(2,1)S(1)} %dynamic-slice_reduce_fusion), kind=kOutput, calls=%fused_computation.3 | convolution fusion | flops 675774464 | bytes 13645824 | tf_op jit(solution)/shard_map/bct,bcd->btd/dot_general | solution.py:525
  227.2 0.0 copy-start.6
  227.2 69.5 %scatter_rows.1 = f32[2,64,2048]{2,1,0:T(8,128)} custom-call(bf16[32,64,2048]{2,1,0:T(8,128)(2,1)} %bitcast.43), custom_call_target="tpu_custom_call" | custom-call | tf_op jit(solution)/shard_map/scatter_rows/pallas_call | solution.py:245
  296.7 1.4 multiply_reduce_fusion
  298.0 0.1 rsqrt.30
  298.1 0.0 copy-done.6
  298.1 2.3 fusion.19
  (7 shorter events, 0.1 us)
Async XLA Ops:
  0.0 39.4 %copy-start = (bf16[512,2048]{1,0:T(8,128)(2,1)S(1)}, bf16[512,2048]{1,0:T(8,128)(2,1)}, u32[]{:S(2)}) copy-start(bf16[512,2048]{1,0:T(8,128)(2,1)} %param.29) | copy-start | bytes 6291460
  39.4 1.8 copy-start.2
  41.3 19.3 %copy-start.3 = (bf16[128,2048]{1,0:T(8,128)(2,1)S(1)}, bf16[128,2048]{1,0:T(8,128)(2,1)}, u32[]{:S(2)}) copy-start(bf16[128,2048]{1,0:T(8,128)(2,1)} %param.31) | copy-start | bytes 1572868
  41.3 19.3 %copy-start.4 = (f32[2048]{0:T(1024)S(1)}, f32[2048]{0:T(1024)}, u32[]{:S(2)}) copy-start(f32[2048]{0:T(1024)} %param.32) | copy-start | bytes 24580
  41.3 20.9 %copy-start.5 = (f32[2048]{0:T(1024)S(1)}, f32[2048]{0:T(1024)}, u32[]{:S(2)}) copy-start(f32[2048]{0:T(1024)} %param.33) | copy-start | bytes 24580
  185.5 7.4 %copy-start.7 = (bf16[1,2048,1024]{2,1,0:T(8,128)(2,1)S(1)}, bf16[1,2048,1024]{2,1,0:T(8,128)(2,1)}, u32[]{:S(2)}) copy-start(bf16[1,2048,1024]{2,1,0:T(8,128)(2,1)} %param.37) | copy-start | bytes 12582916
  190.6 2.4 copy-start.1
  227.2 70.9 %copy-start.6 = (f32[2048]{0:T(1024)S(1)}, f32[2048]{0:T(1024)}, u32[]{:S(2)}) copy-start(f32[2048]{0:T(1024)} %param.34) | copy-start | bytes 24580
